TPU v7x, 32 devices: a whole 2x2x4 slice. The times are simulated.
32 devices in a mesh: sp: 4 (over z), fs: 4 (over y, x), tp: 2 (over core).
Axes of the slice: x: 2, y: 2, z: 4, core: 2. Of those that a mesh axis runs over, the one named last changes fastest.
Arguments:
- tokens: bfloat16 [4, 4096, 2048], P('fs', ('sp', 'tp')), may hold values from -6 to 6
- input_norm_gain: float32 [2048], replicated, may hold values from 0.1 to 1.9
- earlier_gate: bfloat16 [2048, 1024], P(('sp', 'fs'), 'tp'), may hold values from -0.125 to 0.125
- later_gate: bfloat16 [2048, 1024], P(('sp', 'fs'), 'tp'), may hold values from -0.125 to 0.125
- convolution_input: bfloat16 [2048, 1024], P(('sp', 'fs'), 'tp'), may hold values from -0.125 to 0.125
- convolution_taps: float32 [3, 1024], P(None, 'tp'), may hold values from -3 to 3
- receptance: bfloat16 [2048, 1024], P(('sp', 'fs'), 'tp'), may hold values from -0.125 to 0.125
- key_matrix: bfloat16 [2048, 1024], P(('sp', 'fs'), 'tp'), may hold values from -0.125 to 0.125
- value_matrix: bfloat16 [2048, 1024], P(('sp', 'fs'), 'tp'), may hold values from -0.125 to 0.125
- decay_matrix: bfloat16 [2048, 1024], P(('sp', 'fs'), 'tp'), may hold values from -0.125 to 0.125
- rate_matrix: bfloat16 [2048, 1024], P(('sp', 'fs'), 'tp'), may hold values from -0.125 to 0.125
- decay_floor: float32 [1024], P('tp'), may hold values from -16 to -3.4
- rate_offset: float32 [1024], P('tp'), may hold values from -7.5 to 1
- decay_spike: float32 [4, 4096, 1024], P('fs', 'sp', 'tp'), may hold values from -1.3 to 0
- initial_state: float32 [4, 16, 64, 64], P('fs', 'tp'), may hold values from -384 to 384
- head_norm_gain: float32 [1024], P('tp'), may hold values from 0.1 to 1.9
- convolution_output: bfloat16 [1024, 2048], P('tp', ('sp', 'fs')), may hold values from -0.125 to 0.125
- state_heads_output: bfloat16 [1024, 2048], P('tp', ('sp', 'fs')), may hold values from -0.125 to 0.125
Outputs:
- mixed: bfloat16 [4, 4096, 2048], P('fs', ('sp', 'tp'))
All inputs are finite; a program needn't handle non-finite values.
Results may differ from a plain program's by a relative error of at most 0.02.
Values may be sent and summed in bfloat16 or wider, within the bound.
A program may use at most 128 MiB of HBM per device.

v0:
```python
import jax
import jax.numpy as jnp
from jax import lax
from jax.sharding import PartitionSpec as P

HEAD_WIDTH = 64
BLOCK = 64


norm_eps = 1e-06
key_eps = 1e-06
highest = lax.Precision.HIGHEST


def passed_along(block, axis, distance):
    devices = range(lax.axis_size(axis))
    route = [(i - distance, i) for i in devices if i - distance in devices]
    return lax.ppermute(block, axis, route)


def rms_rows(activations, gain_vector):
    values = activations.astype(jnp.float32)
    inv_scale = lax.rsqrt(jnp.mean(values * values, axis=-1, keepdims=True) + norm_eps)
    return (values * inv_scale * gain_vector).astype(jnp.bfloat16)


def project(activations, weight):
    return jnp.dot(activations, weight, preferred_element_type=jnp.float32).astype(jnp.bfloat16)


def conv_branch(pre_values, post_values, conv_values, convolution_taps):
    product = pre_values.astype(jnp.float32) * conv_values.astype(jnp.float32)
    reach_rows = convolution_taps.shape[0] - 1
    sequence_rows = product.shape[0]
    edge_rows = passed_along(product[sequence_rows - reach_rows :], "sp", 1)
    padded = jnp.concatenate([edge_rows, product], axis=0)
    filtered = convolution_taps[0] * padded[0:sequence_rows]
    for offset in range(1, convolution_taps.shape[0]):
        filtered = filtered + convolution_taps[offset] * padded[offset : offset + sequence_rows]
    return (post_values.astype(jnp.float32) * filtered).astype(jnp.bfloat16)


def pairs(left_side, right_side, allowed):
    return jnp.where(
        allowed, jnp.einsum("thj,shj->hts", left_side, right_side, precision=highest), 0.0
    )


def block_pass(carried, inputs):
    queries, key_rows, value_rows, unit_keys, beta_rows, logarithm_decay = inputs
    span_rows = logarithm_decay.shape[0]
    cumulative = jnp.cumsum(logarithm_decay, axis=0)
    previous = cumulative - logarithm_decay
    middle = cumulative[span_rows // 2]
    later_index = lax.broadcasted_iota(jnp.int32, (span_rows, span_rows), 0)
    earlier_index = lax.broadcasted_iota(jnp.int32, (span_rows, span_rows), 1)
    strict = (later_index > earlier_index)[None]
    inclusive = (later_index >= earlier_index)[None]
    ask_keys = unit_keys * jnp.exp(previous - middle)
    ask_reads = queries * jnp.exp(cumulative - middle)
    give_keys = key_rows * jnp.exp(middle - cumulative)
    give_betas = beta_rows * jnp.exp(middle - cumulative)
    key_ask = pairs(ask_keys, give_keys, strict)
    beta_ask = pairs(ask_keys, give_betas, strict)
    key_read = pairs(ask_reads, give_keys, inclusive)
    beta_read = pairs(ask_reads, give_betas, inclusive)
    extended = jnp.concatenate([value_rows, jnp.zeros_like(value_rows)], axis=2)
    from_start = jnp.einsum(
        "thj,hrj->htr", unit_keys * jnp.exp(previous), carried, precision=highest
    )
    right_side = from_start + jnp.einsum("hts,shr->htr", key_ask, extended, precision=highest)
    system = beta_ask + jnp.eye(span_rows, dtype=jnp.float32)[None]
    removed = jax.scipy.linalg.solve_triangular(system, right_side, lower=True, unit_diagonal=True)
    outputs = (
        jnp.einsum("thj,hrj->thr", queries * jnp.exp(cumulative), carried, precision=highest)
        + jnp.einsum("hts,shr->thr", key_read, extended, precision=highest)
        - jnp.einsum("hts,hsr->thr", beta_read, removed, precision=highest)
    )
    closing = cumulative[span_rows - 1]
    tail_decay = jnp.exp(closing - cumulative)
    carried = (
        carried * jnp.exp(closing)[:, None, :]
        + jnp.einsum("shr,shj->hrj", extended, key_rows * tail_decay, precision=highest)
        - jnp.einsum("hsr,shj->hrj", removed, beta_rows * tail_decay, precision=highest)
    )
    return (carried, outputs)


def on_device(
    tokens,
    input_norm_gain,
    earlier_gate,
    later_gate,
    convolution_input,
    convolution_taps,
    receptance,
    key_matrix,
    value_matrix,
    decay_matrix,
    rate_matrix,
    decay_floor,
    rate_offset,
    decay_spike,
    initial_state,
    head_norm_gain,
    convolution_output,
    state_heads_output,
):
    normed = rms_rows(tokens[0], input_norm_gain)
    channels = earlier_gate.shape[1]
    gathered = (
        lax.all_gather(earlier_gate, ("sp", "fs"), axis=0, tiled=True),
        lax.all_gather(later_gate, ("sp", "fs"), axis=0, tiled=True),
        lax.all_gather(convolution_input, ("sp", "fs"), axis=0, tiled=True),
        lax.all_gather(receptance, ("sp", "fs"), axis=0, tiled=True),
        lax.all_gather(key_matrix, ("sp", "fs"), axis=0, tiled=True),
        lax.all_gather(value_matrix, ("sp", "fs"), axis=0, tiled=True),
        lax.all_gather(decay_matrix, ("sp", "fs"), axis=0, tiled=True),
        lax.all_gather(rate_matrix, ("sp", "fs"), axis=0, tiled=True),
    )
    piece = lax.all_gather(normed, "tp", axis=0, tiled=True)
    projected = jnp.concatenate([project(piece, weight) for weight in gathered], axis=1)
    pieces = jnp.split(projected, 8, axis=1)
    conv_mixed = conv_branch(pieces[0], pieces[1], pieces[2], convolution_taps)
    queries_raw, keys_raw, values_raw, decay_pre, rate_pre = pieces[3:]
    sequence_rows = queries_raw.shape[0]
    present_heads = channels // HEAD_WIDTH

    def by_heads(array):
        return array.astype(jnp.float32).reshape(sequence_rows, present_heads, HEAD_WIDTH)

    queries = by_heads(queries_raw)
    key_rows = by_heads(keys_raw)
    value_rows = by_heads(values_raw)
    logarithm_decay = -jnp.exp(
        decay_floor.reshape(present_heads, HEAD_WIDTH) + jnp.tanh(by_heads(decay_pre))
    )
    logarithm_decay = logarithm_decay + decay_spike[0].reshape(
        sequence_rows, present_heads, HEAD_WIDTH
    )
    learn_rate = jax.nn.sigmoid(rate_offset.reshape(present_heads, HEAD_WIDTH) + by_heads(rate_pre))
    unit_keys = key_rows * lax.rsqrt(jnp.sum(key_rows * key_rows, axis=-1, keepdims=True) + key_eps)
    beta_rows = learn_rate * unit_keys
    blocks = sequence_rows // BLOCK

    def in_blocks(array):
        return array.reshape(blocks, BLOCK, present_heads, HEAD_WIDTH)

    identity = jnp.broadcast_to(
        jnp.eye(HEAD_WIDTH, dtype=jnp.float32), (present_heads, HEAD_WIDTH, HEAD_WIDTH)
    )
    initial_rows = jnp.concatenate(
        [jnp.zeros((present_heads, HEAD_WIDTH, HEAD_WIDTH), jnp.float32), identity], axis=1
    )
    ending, outputs = lax.scan(
        block_pass,
        initial_rows,
        tuple(
            (
                in_blocks(array)
                for array in (queries, key_rows, value_rows, unit_keys, beta_rows, logarithm_decay)
            )
        ),
    )
    outputs = outputs.reshape(sequence_rows, present_heads, 2 * HEAD_WIDTH)
    carry_source = ending[:, :HEAD_WIDTH, :]
    carry_map = ending[:, HEAD_WIDTH:, :]
    first_state = initial_state[0]
    is_first = lax.axis_index("sp") == 0

    def relay_turn(turn, received):
        current = jnp.where(is_first, first_state, received)
        passed = jnp.einsum("hvj,hjk->hvk", current, carry_map, precision=highest) + carry_source
        return passed_along(passed.astype(jnp.bfloat16), "sp", 1).astype(passed.dtype)

    received = lax.fori_loop(0, lax.axis_size("sp") - 1, relay_turn, jnp.zeros_like(first_state))
    opening_state = jnp.where(is_first, first_state, received)
    reads = outputs[..., :HEAD_WIDTH] + jnp.einsum(
        "thj,hvj->thv", outputs[..., HEAD_WIDTH:], opening_state, precision=highest
    )
    centered = reads - jnp.mean(reads, axis=-1, keepdims=True)
    variance = jnp.mean(centered * centered, axis=-1, keepdims=True)
    state_mixed = (
        centered
        * lax.rsqrt(variance + HEAD_WIDTH * 1e-05)
        * head_norm_gain.reshape(present_heads, HEAD_WIDTH)
    )
    state_mixed = state_mixed.reshape(sequence_rows, channels).astype(jnp.bfloat16)
    conv_whole, state_whole = (
        lax.all_gather(convolution_output, ("sp", "fs"), axis=1, tiled=True),
        lax.all_gather(state_heads_output, ("sp", "fs"), axis=1, tiled=True),
    )
    mixed = lax.psum_scatter(
        (
            jnp.dot(conv_mixed, conv_whole, preferred_element_type=jnp.float32)
            + jnp.dot(state_mixed, state_whole, preferred_element_type=jnp.float32)
        ).astype(jnp.bfloat16),
        "tp",
        scatter_dimension=0,
        tiled=True,
    )
    return mixed[None]


def solution(mesh):
    placed = (
        P("fs", ("sp", "tp"), None),
        P(),
        P(("sp", "fs"), "tp"),
        P(("sp", "fs"), "tp"),
        P(("sp", "fs"), "tp"),
        P(None, "tp"),
        P(("sp", "fs"), "tp"),
        P(("sp", "fs"), "tp"),
        P(("sp", "fs"), "tp"),
        P(("sp", "fs"), "tp"),
        P(("sp", "fs"), "tp"),
        P("tp"),
        P("tp"),
        P("fs", "sp", "tp"),
        P("fs", "tp", None, None),
        P("tp"),
        P("tp", ("sp", "fs")),
        P("tp", ("sp", "fs")),
    )
    return jax.shard_map(
        on_device,
        mesh=mesh,
        in_specs=placed,
        out_specs=P("fs", ("sp", "tp"), None),
        check_vma=False,
    )
```

profile of v0, /device:TPU:0, one launch (start us, length us, event | category | flops | bytes accessed | tf_op | source)
XLA Modules:
  0.0 1277.1 jit_solution(8981503472595466093)
XLA Ops:
  7.3 2.1 fusion.40
  9.4 1.9 fusion.42
  17.5 2.4 reshape_squeeze.3
  20.3 53.0 %all-gather.26.cloned.1.call-done = bf16[2048,512]{1,0:T(8,128)(2,1)} async-done(((bf16[128,512]{1,0:T(8,128)(2,1)}), bf16[2048,512]{1,0:T(8,128)(2,1)}) %all-gather.26.cloned.1.call-update) | async-done | bytes 2097168 | tf_op jit(solution)/shard_map/all_gather | solution.py:116
  73.2 14.0 %all-gather.12.cloned.1.call-done = bf16[1024,2048]{1,0:T(8,128)(2,1)} async-done(((bf16[512,2048]{1,0:T(8,128)(2,1)}), bf16[1024,2048]{1,0:T(8,128)(2,1)}) %all-gather.12.cloned.1.call-update) | async-done | bytes 4194320 | tf_op jit(solution)/shard_map/all_gather | solution.py:121
  87.3 5.3 bitcast_reduce_fusion
  92.5 2.5 reshape_reshape.17
  95.0 4.4 copy.61
  99.6 52.0 %all-gather.28.cloned.1.call-done = bf16[2048,512]{1,0:T(8,128)(2,1)} async-done(((bf16[128,512]{1,0:T(8,128)(2,1)}), bf16[2048,512]{1,0:T(8,128)(2,1)}) %all-gather.28.cloned.1.call-update) | async-done | bytes 2097168 | tf_op jit(solution)/shard_map/all_gather | solution.py:119
  151.6 5.2 fusion.55
  156.8 2.5 reshape.102
  159.3 54.2 %all-gather.22.cloned.1.call-done = bf16[2048,512]{1,0:T(8,128)(2,1)} async-done(((bf16[128,512]{1,0:T(8,128)(2,1)}), bf16[2048,512]{1,0:T(8,128)(2,1)}) %all-gather.22.cloned.1.call-update) | async-done | bytes 2097168 | tf_op jit(solution)/shard_map/all_gather | solution.py:118
  213.5 5.2 convert_tanh_fusion
  218.7 2.5 tanh.8
  221.1 54.2 %all-gather.24.cloned.1.call-done = bf16[2048,512]{1,0:T(8,128)(2,1)} async-done(((bf16[128,512]{1,0:T(8,128)(2,1)}), bf16[2048,512]{1,0:T(8,128)(2,1)}) %all-gather.24.cloned.1.call-update) | async-done | bytes 2097168 | tf_op jit(solution)/shard_map/all_gather | solution.py:117
  275.3 5.2 fusion.57
  280.5 2.4 reshape.100
  282.9 54.3 %all-gather.30.cloned.1.call-done = bf16[2048,512]{1,0:T(8,128)(2,1)} async-done(((bf16[128,512]{1,0:T(8,128)(2,1)}), bf16[2048,512]{1,0:T(8,128)(2,1)}) %all-gather.30.cloned.1.call-update) | async-done | bytes 2097168 | tf_op jit(solution)/shard_map/all_gather | solution.py:115
  337.1 5.2 fusion.54
  342.3 2.6 reshape.103
  344.9 6.6 negate_add_fusion
  352.5 4.0 divide_multiply_fusion
  356.5 825.0 %while.23 = (s32[]{:T(128)}, f32[8,128,64]{1,2,0:T(8,128)S(1)}, f32[16,64,8,128]{3,2,1,0:T(8,128)}, f32[16,64,8,64]{3,2,1,0:T(8,128)}, f32[16,64,8,64]{3,2,1,0:T...) while((s32[]{:T(128)}, f32[8,128,64]{1,2,0:T(8,128)S(1)}, ...), condition=%wide.region_4.5_spmd, body=%wide.region_2.4_spmd.sunk | while | flops 506458176 | bytes 11128429 | solution.py:155
  357.5 1.5 bitcast_multiply_fusion.9
  362.9 40.0 %custom-call.7 = f32[8,1,64,64]{2,3,1,0:T(8,128)S(1)} custom-call(f32[8,1,64,64]{3,2,1,0:T(8,128)} %fusion.160), custom_call_target="InvertDiagBlocksLowerTriangular" | custom-call | tf_op jit(solution)/shard_map/while/body/eval_jaxpr/jit(_solve_triangular)/vmap()/triangular_solve | solution.py:73
  409.1 1.5 bitcast_multiply_fusion.9
  414.5 40.0 %custom-call.7 = f32[8,1,64,64]{2,3,1,0:T(8,128)S(1)} custom-call(f32[8,1,64,64]{3,2,1,0:T(8,128)} %fusion.160), custom_call_target="InvertDiagBlocksLowerTriangular" | custom-call | tf_op jit(solution)/shard_map/while/body/eval_jaxpr/jit(_solve_triangular)/vmap()/triangular_solve | solution.py:73
  460.7 1.5 bitcast_multiply_fusion.9
  466.0 40.1 %custom-call.7 = f32[8,1,64,64]{2,3,1,0:T(8,128)S(1)} custom-call(f32[8,1,64,64]{3,2,1,0:T(8,128)} %fusion.160), custom_call_target="InvertDiagBlocksLowerTriangular" | custom-call | tf_op jit(solution)/shard_map/while/body/eval_jaxpr/jit(_solve_triangular)/vmap()/triangular_solve | solution.py:73
  512.2 1.5 bitcast_multiply_fusion.9
  517.6 40.0 %custom-call.7 = f32[8,1,64,64]{2,3,1,0:T(8,128)S(1)} custom-call(f32[8,1,64,64]{3,2,1,0:T(8,128)} %fusion.160), custom_call_target="InvertDiagBlocksLowerTriangular" | custom-call | tf_op jit(solution)/shard_map/while/body/eval_jaxpr/jit(_solve_triangular)/vmap()/triangular_solve | solution.py:73
  563.8 1.5 bitcast_multiply_fusion.9
  569.2 40.1 %custom-call.7 = f32[8,1,64,64]{2,3,1,0:T(8,128)S(1)} custom-call(f32[8,1,64,64]{3,2,1,0:T(8,128)} %fusion.160), custom_call_target="InvertDiagBlocksLowerTriangular" | custom-call | tf_op jit(solution)/shard_map/while/body/eval_jaxpr/jit(_solve_triangular)/vmap()/triangular_solve | solution.py:73
  615.4 1.6 bitcast_multiply_fusion.9
  620.8 40.0 %custom-call.7 = f32[8,1,64,64]{2,3,1,0:T(8,128)S(1)} custom-call(f32[8,1,64,64]{3,2,1,0:T(8,128)} %fusion.160), custom_call_target="InvertDiagBlocksLowerTriangular" | custom-call | tf_op jit(solution)/shard_map/while/body/eval_jaxpr/jit(_solve_triangular)/vmap()/triangular_solve | solution.py:73
  667.0 1.5 bitcast_multiply_fusion.9
  672.3 40.0 %custom-call.7 = f32[8,1,64,64]{2,3,1,0:T(8,128)S(1)} custom-call(f32[8,1,64,64]{3,2,1,0:T(8,128)} %fusion.160), custom_call_target="InvertDiagBlocksLowerTriangular" | custom-call | tf_op jit(solution)/shard_map/while/body/eval_jaxpr/jit(_solve_triangular)/vmap()/triangular_solve | solution.py:73
  718.5 1.5 bitcast_multiply_fusion.9
  723.9 40.0 %custom-call.7 = f32[8,1,64,64]{2,3,1,0:T(8,128)S(1)} custom-call(f32[8,1,64,64]{3,2,1,0:T(8,128)} %fusion.160), custom_call_target="InvertDiagBlocksLowerTriangular" | custom-call | tf_op jit(solution)/shard_map/while/body/eval_jaxpr/jit(_solve_triangular)/vmap()/triangular_solve | solution.py:73
  775.5 40.0 %custom-call.7 = f32[8,1,64,64]{2,3,1,0:T(8,128)S(1)} custom-call(f32[8,1,64,64]{3,2,1,0:T(8,128)} %fusion.160), custom_call_target="InvertDiagBlocksLowerTriangular" | custom-call | tf_op jit(solution)/shard_map/while/body/eval_jaxpr/jit(_solve_triangular)/vmap()/triangular_solve | solution.py:73
  821.6 1.5 bitcast_multiply_fusion.9
  827.0 40.0 %custom-call.7 = f32[8,1,64,64]{2,3,1,0:T(8,128)S(1)} custom-call(f32[8,1,64,64]{3,2,1,0:T(8,128)} %fusion.160), custom_call_target="InvertDiagBlocksLowerTriangular" | custom-call | tf_op jit(solution)/shard_map/while/body/eval_jaxpr/jit(_solve_triangular)/vmap()/triangular_solve | solution.py:73
  878.6 40.0 %custom-call.7 = f32[8,1,64,64]{2,3,1,0:T(8,128)S(1)} custom-call(f32[8,1,64,64]{3,2,1,0:T(8,128)} %fusion.160), custom_call_target="InvertDiagBlocksLowerTriangular" | custom-call | tf_op jit(solution)/shard_map/while/body/eval_jaxpr/jit(_solve_triangular)/vmap()/triangular_solve | solution.py:73
  930.1 40.0 %custom-call.7 = f32[8,1,64,64]{2,3,1,0:T(8,128)S(1)} custom-call(f32[8,1,64,64]{3,2,1,0:T(8,128)} %fusion.160), custom_call_target="InvertDiagBlocksLowerTriangular" | custom-call | tf_op jit(solution)/shard_map/while/body/eval_jaxpr/jit(_solve_triangular)/vmap()/triangular_solve | solution.py:73
  981.7 40.0 %custom-call.7 = f32[8,1,64,64]{2,3,1,0:T(8,128)S(1)} custom-call(f32[8,1,64,64]{3,2,1,0:T(8,128)} %fusion.160), custom_call_target="InvertDiagBlocksLowerTriangular" | custom-call | tf_op jit(solution)/shard_map/while/body/eval_jaxpr/jit(_solve_triangular)/vmap()/triangular_solve | solution.py:73
  1033.2 40.0 %custom-call.7 = f32[8,1,64,64]{2,3,1,0:T(8,128)S(1)} custom-call(f32[8,1,64,64]{3,2,1,0:T(8,128)} %fusion.160), custom_call_target="InvertDiagBlocksLowerTriangular" | custom-call | tf_op jit(solution)/shard_map/while/body/eval_jaxpr/jit(_solve_triangular)/vmap()/triangular_solve | solution.py:73
  1084.8 40.0 %custom-call.7 = f32[8,1,64,64]{2,3,1,0:T(8,128)S(1)} custom-call(f32[8,1,64,64]{3,2,1,0:T(8,128)} %fusion.160), custom_call_target="InvertDiagBlocksLowerTriangular" | custom-call | tf_op jit(solution)/shard_map/while/body/eval_jaxpr/jit(_solve_triangular)/vmap()/triangular_solve | solution.py:73
  1136.4 40.0 %custom-call.7 = f32[8,1,64,64]{2,3,1,0:T(8,128)S(1)} custom-call(f32[8,1,64,64]{3,2,1,0:T(8,128)} %fusion.160), custom_call_target="InvertDiagBlocksLowerTriangular" | custom-call | tf_op jit(solution)/shard_map/while/body/eval_jaxpr/jit(_solve_triangular)/vmap()/triangular_solve | solution.py:73
  1182.5 7.8 fusion.64
  1190.3 3.0 copy.72
  1193.4 6.2 convolution_convert_fusion.6
  1199.6 5.5 convert_multiply_fusion.2
  1205.1 3.3 collective-permute-start.1
  1208.5 20.2 %while.24 = (s32[]{:T(128)}, f32[8,64,64]{2,1,0:T(8,128)S(1)}, pred[]{:T(512)}, f32[8,64,64]{2,1,0:T(8,128)S(1)}, f32[8,64,64]{2,1,0:T(8,128)S(1)}, /*index=5*/f32[8,64,64]{2,1,0:T(8,128)S(1)}, s32[]{:T(128)}, s32[]{:T(128)}) while((s32[]{:T(128)}, f32[8,64,64]{2,1,0:T(8,128)S(1)}, pred[]{:T(512)}, f32[8,64,64]{2,1,0:T(8,128)S(1)}, ...), condition=%wide.region_6.7_spmd.clone, body=%wide.region_5.6_spmd.clone.sunk | while | flops 25329668 | bytes 1048712 | solution.py:176
  1208.9 2.6 collective-permute-start
  1211.6 2.5 collective-permute-done
  1214.5 4.4 collective-permute-start
  1218.9 2.5 collective-permute-done
  1221.8 4.4 collective-permute-start
  1226.2 2.5 collective-permute-done
  1228.7 7.4 fusion.67
  1238.1 11.5 fusion.58
  1249.6 8.4 add_convert_fusion
  1258.0 11.8 reduce-scatter.2.cloned.1.call-done
  (440 shorter events, 181.2 us)
Async XLA Ops:
  6.5 2.9 copy-start.3
  6.5 2.9 copy-start.6
  6.5 66.7 %all-gather.26.cloned.1.call-start = ((), (), s32[]{:S(2)}) async-start(), calls=%async_computation.8 | async-start | bytes 2228224 | tf_op jit(solution)/shard_map/all_gather | solution.py:116
  7.3 80.0 %all-gather.12.cloned.1.call-start = ((), (), s32[]{:S(2)}) async-start(), calls=%async_computation.1 | async-start | bytes 6291456 | tf_op jit(solution)/shard_map/all_gather | solution.py:121
  11.3 6.1 copy-start.8
  11.3 6.2 copy-start.4
  11.3 140.3 %all-gather.28.cloned.1.call-start = ((), (), s32[]{:S(2)}) async-start(), calls=%async_computation.9 | async-start | bytes 2228224 | tf_op jit(solution)/shard_map/all_gather | solution.py:119
  12.0 201.4 %all-gather.22.cloned.1.call-start = ((), (), s32[]{:S(2)}) async-start(), calls=%async_computation.6 | async-start | bytes 2228224 | tf_op jit(solution)/shard_map/all_gather | solution.py:118
  12.6 262.7 %all-gather.24.cloned.1.call-start = ((), (), s32[]{:S(2)}) async-start(), calls=%async_computation.7 | async-start | bytes 2228224 | tf_op jit(solution)/shard_map/all_gather | solution.py:117
  13.2 323.9 %all-gather.30.cloned.1.call-start = ((), (), s32[]{:S(2)}) async-start(), calls=%async_computation.10 | async-start | bytes 2228224 | tf_op jit(solution)/shard_map/all_gather | solution.py:115
  13.8 1179.6 %all-gather.16.cloned.1.call-start = ((), (), s32[]{:S(2)}) async-start(), calls=%async_computation.3 | async-start | bytes 2228224 | tf_op jit(solution)/shard_map/all_gather | solution.py:112
  14.5 1185.1 %all-gather.18.cloned.1.call-start = ((), (), s32[]{:S(2)}) async-start(), calls=%async_computation.4 | async-start | bytes 2228224 | tf_op jit(solution)/shard_map/all_gather | solution.py:114
  15.3 1221.7 %all-gather.14.cloned.1.call-start = ((), (), s32[]{:S(2)}) async-start(), calls=%async_computation.2 | async-start | bytes 2228224 | tf_op jit(solution)/shard_map/all_gather | solution.py:113
  16.0 1221.0 %all-gather.20.cloned.1.call-start = ((), (), s32[]{:S(2)}) async-start(), calls=%async_computation.5 | async-start | bytes 2228224 | tf_op jit(solution)/shard_map/all_gather | solution.py:190
  16.6 1233.0 %all-gather.32.cloned.1.call-start = ((), (), s32[]{:S(2)}) async-start(), calls=%async_computation.11 | async-start | bytes 2228224 | tf_op jit(solution)/shard_map/all_gather | solution.py:191
  17.3 1252.5 %reduce-scatter.2.cloned.1.call-start = ((), (), s32[]{:S(2)}) async-start(), calls=%async_computation.12 | async-start | bytes 6291456 | tf_op jit(solution)/shard_map/reduce_scatter | solution.py:193
  17.5 2.4 copy-start.9
  17.5 2.5 copy-start.10
  17.5 2.6 copy-start.7
  344.9 6.6 copy-start
  344.9 7.6 copy-start.1
  1199.6 8.9 copy-start.2
  1199.6 8.8 copy-start.5
  1205.1 3.4 copy-start.11
  1205.1 31.9 %collective-permute-start.1 = (f32[2,512]{1,0:T(2,128)S(1)}, f32[2,512]{1,0:T(2,128)S(1)}, u32[]{:S(2)}, u32[]{:S(2)}) collective-permute-start(f32[2,512]{1,0:T(2,128)S(1)} %slice.54), channel_id=1, source_target_pairs={{0,8},{8,16},{16,24},{1,9},{9,17},{17,25},{2,10},{10,18},{18,26},{... | collective-permute-start | bytes 12296 | tf_op jit(solution)/shard_map/ppermute | solution.py:18
  1208.9 5.1 collective-permute-start
  1214.5 6.9 collective-permute-start
  1221.8 6.9 collective-permute-start
  1236.5 1.6 copy-start.12
Sparse Core Ops, SparseCore 0:
  10.1 63.0 all-gather.25
  74.8 12.4 all-gather.11
  90.0 61.5 all-gather.27
  154.3 59.1 all-gather.21
  216.1 59.1 all-gather.23
  277.9 59.1 all-gather.29
  339.9 60.5 all-gather.15
  403.3 60.3 all-gather.17
  466.5 60.9 all-gather.13
  530.0 63.1 all-gather.19
  595.9 63.2 all-gather.31
  1258.2 11.6 reduce-scatter.1
where the time goes:
time: 1290 us; the launch traced here: 1280 us
  other arithmetic  698 us (54%)
  waiting for transfers between devices  307 us (24%)
  matrix products  176 us (14%)
  local copies, waits for them, and re-layouts  64.2 us (5%)
  starting transfers between devices  15.1 us (1%)
  between operations  14.2 us (1%)
    another operation x32, other arithmetic, block_pass(): jax.scipy.linalg.solve_triangular(system, right_side, lower=True, unit_di...  641 us
    all_gather x1, waiting for transfers between devices, on_device(): lax.all_gather(receptance, ('sp', 'fs'), axis=0, tiled=True)  54.3 us
    all_gather x1, waiting for transfers between devices, on_device(): lax.all_gather(decay_matrix, ('sp', 'fs'), axis=0, tiled=True)  54.2 us
    all_gather x1, waiting for transfers between devices, on_device(): lax.all_gather(value_matrix, ('sp', 'fs'), axis=0, tiled=True)  54.2 us
    all_gather x1, waiting for transfers between devices, on_device(): lax.all_gather(key_matrix, ('sp', 'fs'), axis=0, tiled=True)  53 us
    all_gather x1, waiting for transfers between devices, on_device(): lax.all_gather(rate_matrix, ('sp', 'fs'), axis=0, tiled=True)  52 us
    dot_general x64, matrix products, pairs(): jnp.einsum('thj,shj->hts', left_side, right_side, precision=highest)  49.8 us
    dot_general x7, matrix products, project(): jnp.dot(activations, weight, preferred_element_type=jnp.float32)  37.6 us
  transfers between devices with their start and end apart: 16, of which 10 were waited for; matrix products, arithmetic and copies ran while one was open for 73% of the time, Pallas kernels for 0%

commit v1 on v0

v1 whole, which is shorter than its diff:
```python
import jax
import jax.numpy as jnp
from jax import lax
from jax.experimental import pallas as pl
from jax.experimental.pallas import tpu as pltpu
from jax.sharding import PartitionSpec as P

HEAD_WIDTH = 64
BLOCK = 64


norm_eps = 1e-06
key_eps = 1e-06
highest = lax.Precision.HIGHEST


def passed_along(block, axis, distance):
    devices = range(lax.axis_size(axis))
    route = [(i - distance, i) for i in devices if i - distance in devices]
    return lax.ppermute(block, axis, route)


def rms_rows(activations, gain_vector):
    values = activations.astype(jnp.float32)
    inv_scale = lax.rsqrt(jnp.mean(values * values, axis=-1, keepdims=True) + norm_eps)
    return (values * inv_scale * gain_vector).astype(jnp.bfloat16)


def project(activations, weight):
    return jnp.dot(activations, weight, preferred_element_type=jnp.float32).astype(jnp.bfloat16)


def conv_branch(pre_values, post_values, conv_values, convolution_taps):
    product = pre_values.astype(jnp.float32) * conv_values.astype(jnp.float32)
    reach_rows = convolution_taps.shape[0] - 1
    sequence_rows = product.shape[0]
    edge_rows = passed_along(product[sequence_rows - reach_rows :], "sp", 1)
    padded = jnp.concatenate([edge_rows, product], axis=0)
    filtered = convolution_taps[0] * padded[0:sequence_rows]
    for offset in range(1, convolution_taps.shape[0]):
        filtered = filtered + convolution_taps[offset] * padded[offset : offset + sequence_rows]
    return (post_values.astype(jnp.float32) * filtered).astype(jnp.bfloat16)


def dot_bf16(left, right, contract):
    return lax.dot_general(
        left.astype(jnp.bfloat16),
        right.astype(jnp.bfloat16),
        (contract, ((), ())),
        preferred_element_type=jnp.float32,
    )


ROWS = ((1,), (0,))
TRANSPOSED_RIGHT = ((1,), (1,))
TRANSPOSED_LEFT = ((0,), (0,))


def split_dot(exact, wide, contract, left_exact):
    total = None
    rest = wide
    for _ in range(3):
        part = rest.astype(jnp.bfloat16)
        rest = rest - part.astype(jnp.float32)
        piece = (
            dot_bf16(exact, part, contract) if left_exact else dot_bf16(part, exact, contract)
        )
        total = piece if total is None else total + piece
    return total


def unit_inverse(lower, row, col, size):
    inverse = jnp.where(row == col, 1.0, 0.0) - jnp.where(
        ((row ^ col) == 1) & (row > col), lower, 0.0
    )
    width = 2
    while width < size:
        cross = ((row // (2 * width)) == (col // (2 * width))) & (
            (row // width) > (col // width)
        )
        step = dot_bf16(jnp.where(cross, lower, 0.0), inverse, ROWS)
        inverse = inverse - dot_bf16(inverse, step, ROWS)
        width *= 2
    return inverse


def delta_kernel(proj_ref, spike_ref, floor_ref, offset_ref, reads_ref, maps_ref, ending_ref, state):
    chunk = pl.program_id(0)
    channels = floor_ref.shape[1]
    span = spike_ref.shape[0]
    lanes = 2 * HEAD_WIDTH
    groups = channels // lanes

    @pl.when(chunk == 0)
    def _():
        row = lax.broadcasted_iota(jnp.int32, (2 * lanes, lanes), 0)
        col = lax.broadcasted_iota(jnp.int32, (2 * lanes, lanes), 1)
        start = jnp.where(row - lanes == col, 1.0, 0.0)
        for group in range(groups):
            state[group] = start

    def part(index):
        return proj_ref[:, index * channels : (index + 1) * channels].astype(jnp.float32)

    queries, keys, values, decay_pre, rate_pre = [part(i) for i in range(5)]
    log_decay = -jnp.exp(floor_ref[...] + jnp.tanh(decay_pre)) + spike_ref[...]
    rate = jax.nn.sigmoid(offset_ref[...] + rate_pre)
    tri = lax.broadcasted_iota(jnp.int32, (span, span), 0) >= lax.broadcasted_iota(
        jnp.int32, (span, span), 1
    )
    cumulative = split_dot(jnp.where(tri, 1.0, 0.0), log_decay, ROWS, True)
    previous = cumulative - log_decay
    middle = cumulative[span // 2 : span // 2 + 1]
    closing = cumulative[span - 1 : span]
    square = lax.broadcasted_iota(jnp.int32, (lanes, lanes), 0)
    across = lax.broadcasted_iota(jnp.int32, (lanes, lanes), 1)
    same_head = jnp.where((square // HEAD_WIDTH) == (across // HEAD_WIDTH), 1.0, 0.0)
    first_lanes = lax.broadcasted_iota(jnp.int32, (span, lanes), 1) < HEAD_WIDTH

    def by_head(array):
        return jnp.concatenate(
            [jnp.where(first_lanes, array, 0.0), jnp.where(first_lanes, 0.0, array)], axis=0
        ).astype(jnp.bfloat16)

    grow = jnp.exp(middle - cumulative)
    shrink_previous = jnp.exp(previous - middle)
    shrink = jnp.exp(cumulative - middle)
    from_previous = jnp.exp(previous)
    from_current = jnp.exp(cumulative)
    tail = jnp.exp(closing - cumulative)
    whole = jnp.exp(closing)
    strict = square > across
    inclusive = square >= across
    for group in range(groups):
        cols = slice(group * lanes, (group + 1) * lanes)
        key = keys[:, cols]
        query = queries[:, cols]
        square_sum = split_dot(same_head, key * key, ROWS, False)
        unit = key * lax.rsqrt(square_sum + key_eps)
        beta = rate[:, cols] * unit
        value = by_head(values[:, cols])
        asks = jnp.concatenate(
            [by_head(unit * shrink_previous[:, cols]), by_head(query * shrink[:, cols])], axis=0
        )
        gives = jnp.concatenate(
            [by_head(key * grow[:, cols]), by_head(beta * grow[:, cols])], axis=0
        )
        grams = dot_bf16(asks, gives, TRANSPOSED_RIGHT)
        key_ask = jnp.where(strict, grams[:lanes, :lanes], 0.0)
        beta_ask = jnp.where(strict, grams[:lanes, lanes:], 0.0)
        key_read = jnp.where(inclusive, grams[lanes:, :lanes], 0.0)
        beta_read = jnp.where(inclusive, grams[lanes:, lanes:], 0.0)
        inverse = unit_inverse(beta_ask, square, across, span)
        carried = state[group]
        openers = jnp.concatenate(
            [by_head(unit * from_previous[:, cols]), by_head(query * from_current[:, cols])],
            axis=0,
        )
        opened = dot_bf16(openers, carried, TRANSPOSED_RIGHT)
        inner = dot_bf16(jnp.concatenate([key_ask, key_read], axis=0), value, ROWS)
        right_side = jnp.concatenate(
            [opened[:lanes, :lanes] + inner[:lanes], opened[:lanes, lanes:]], axis=1
        )
        removed = dot_bf16(inverse, right_side, ROWS)
        taken = dot_bf16(beta_read, removed, ROWS)
        out_source = opened[lanes:, :lanes] + inner[lanes:] - taken[:, :lanes]
        out_map = opened[lanes:, lanes:] - taken[:, lanes:]
        reads_ref[:, cols] = out_source[:span] + out_source[span:]
        maps_ref[:, cols] = (out_map[:span] + out_map[span:]).astype(maps_ref.dtype)
        tails = jnp.concatenate(
            [by_head(key * tail[:, cols]), by_head(beta * tail[:, cols])], axis=0
        )
        lefts = jnp.concatenate(
            [
                jnp.concatenate([value, jnp.zeros_like(value)], axis=1),
                (-removed).astype(jnp.bfloat16),
            ],
            axis=0,
        )
        carried = carried * whole[:, cols] + dot_bf16(lefts, tails, TRANSPOSED_LEFT)
        state[group] = carried

    @pl.when(chunk == pl.num_programs(0) - 1)
    def _():
        ending_ref[...] = state[...]


def delta_mix(projected, spike, floor, offset):
    rows, channels = spike.shape
    lanes = 2 * HEAD_WIDTH
    groups = channels // lanes
    wide = projected.shape[1]
    return pl.pallas_call(
        delta_kernel,
        grid=(rows // BLOCK,),
        in_specs=[
            pl.BlockSpec((BLOCK, wide), lambda i: (i, 0)),
            pl.BlockSpec((BLOCK, channels), lambda i: (i, 0)),
            pl.BlockSpec((1, channels), lambda i: (0, 0)),
            pl.BlockSpec((1, channels), lambda i: (0, 0)),
        ],
        out_specs=[
            pl.BlockSpec((BLOCK, channels), lambda i: (i, 0)),
            pl.BlockSpec((BLOCK, channels), lambda i: (i, 0)),
            pl.BlockSpec((groups, 2 * lanes, lanes), lambda i: (0, 0, 0)),
        ],
        out_shape=[
            jax.ShapeDtypeStruct((rows, channels), jnp.float32),
            jax.ShapeDtypeStruct((rows, channels), jnp.bfloat16),
            jax.ShapeDtypeStruct((groups, 2 * lanes, lanes), jnp.float32),
        ],
        scratch_shapes=[pltpu.VMEM((groups, 2 * lanes, lanes), jnp.float32)],
        cost_estimate=pl.CostEstimate(
            flops=40 * rows * channels * lanes, bytes_accessed=20 * rows * channels, transcendentals=0
        ),
    )(projected, spike, floor.reshape(1, channels), offset.reshape(1, channels))


def apart(pair_blocks):
    groups = pair_blocks.shape[0]
    blocks = pair_blocks.reshape(groups, 2, HEAD_WIDTH, 2, HEAD_WIDTH)
    kept = jnp.stack([blocks[:, 0, :, 0], blocks[:, 1, :, 1]], axis=1)
    return kept.reshape(2 * groups, HEAD_WIDTH, HEAD_WIDTH)


def paired(heads):
    groups = heads.shape[0] // 2
    pairs = heads.reshape(groups, 2, HEAD_WIDTH, HEAD_WIDTH)
    zeros = jnp.zeros_like(pairs[:, 0])
    return jnp.concatenate(
        [
            jnp.concatenate([pairs[:, 0], zeros], axis=2),
            jnp.concatenate([zeros, pairs[:, 1]], axis=2),
        ],
        axis=1,
    )


def on_device(
    tokens,
    input_norm_gain,
    earlier_gate,
    later_gate,
    convolution_input,
    convolution_taps,
    receptance,
    key_matrix,
    value_matrix,
    decay_matrix,
    rate_matrix,
    decay_floor,
    rate_offset,
    decay_spike,
    initial_state,
    head_norm_gain,
    convolution_output,
    state_heads_output,
):
    normed = rms_rows(tokens[0], input_norm_gain)
    channels = earlier_gate.shape[1]
    state_weights = jnp.concatenate(
        [receptance, key_matrix, value_matrix, decay_matrix, rate_matrix], axis=1
    )
    conv_weights = jnp.concatenate([earlier_gate, later_gate, convolution_input], axis=1)
    piece = lax.all_gather(normed, "tp", axis=0, tiled=True)
    projected = project(piece, lax.all_gather(state_weights, ("sp", "fs"), axis=0, tiled=True))
    sequence_rows = projected.shape[0]
    present_heads = channels // HEAD_WIDTH
    source_reads, map_reads, ending = delta_mix(projected, decay_spike[0], decay_floor, rate_offset)
    conv_projected = project(
        piece, lax.all_gather(conv_weights, ("sp", "fs"), axis=0, tiled=True)
    )
    pieces = jnp.split(conv_projected, 3, axis=1)
    conv_mixed = conv_branch(pieces[0], pieces[1], pieces[2], convolution_taps)
    lanes = 2 * HEAD_WIDTH
    carry_source = apart(ending[:, :lanes])
    carry_map = apart(ending[:, lanes:])
    first_state = initial_state[0]
    is_first = lax.axis_index("sp") == 0

    def relay_turn(turn, received):
        current = jnp.where(is_first, first_state, received)
        passed = jnp.einsum("hvj,hjk->hvk", current, carry_map, precision=highest) + carry_source
        return passed_along(passed.astype(jnp.bfloat16), "sp", 1).astype(passed.dtype)

    received = lax.fori_loop(0, lax.axis_size("sp") - 1, relay_turn, jnp.zeros_like(first_state))
    opening_state = jnp.where(is_first, first_state, received)
    groups = present_heads // 2
    reads = source_reads.reshape(sequence_rows, groups, lanes) + jnp.einsum(
        "tgj,gvj->tgv",
        map_reads.reshape(sequence_rows, groups, lanes),
        paired(opening_state).astype(jnp.bfloat16),
        preferred_element_type=jnp.float32,
    )
    reads = reads.reshape(sequence_rows, present_heads, HEAD_WIDTH)
    centered = reads - jnp.mean(reads, axis=-1, keepdims=True)
    variance = jnp.mean(centered * centered, axis=-1, keepdims=True)
    state_mixed = (
        centered
        * lax.rsqrt(variance + HEAD_WIDTH * 1e-05)
        * head_norm_gain.reshape(present_heads, HEAD_WIDTH)
    )
    state_mixed = state_mixed.reshape(sequence_rows, channels).astype(jnp.bfloat16)
    conv_whole, state_whole = (
        lax.all_gather(convolution_output, ("sp", "fs"), axis=1, tiled=True),
        lax.all_gather(state_heads_output, ("sp", "fs"), axis=1, tiled=True),
    )
    mixed = lax.psum_scatter(
        (
            jnp.dot(conv_mixed, conv_whole, preferred_element_type=jnp.float32)
            + jnp.dot(state_mixed, state_whole, preferred_element_type=jnp.float32)
        ).astype(jnp.bfloat16),
        "tp",
        scatter_dimension=0,
        tiled=True,
    )
    return mixed[None]


def solution(mesh):
    placed = (
        P("fs", ("sp", "tp"), None),
        P(),
        P(("sp", "fs"), "tp"),
        P(("sp", "fs"), "tp"),
        P(("sp", "fs"), "tp"),
        P(None, "tp"),
        P(("sp", "fs"), "tp"),
        P(("sp", "fs"), "tp"),
        P(("sp", "fs"), "tp"),
        P(("sp", "fs"), "tp"),
        P(("sp", "fs"), "tp"),
        P("tp"),
        P("tp"),
        P("fs", "sp", "tp"),
        P("fs", "tp", None, None),
        P("tp"),
        P("tp", ("sp", "fs")),
        P("tp", ("sp", "fs")),
    )
    return jax.shard_map(
        on_device,
        mesh=mesh,
        in_specs=placed,
        out_specs=P("fs", ("sp", "tp"), None),
        check_vma=False,
    )
```

time: 1290 us -> 523 us (0.41)
  other arithmetic: 698 us -> 6.17 us
  matrix products: 176 us -> 46.2 us
  Pallas kernels: 0 us -> 128 us
  local copies, waits for them, and re-layouts: 64.2 us -> 7.99 us
    another operation x48 -> x3, other arithmetic: 657 us -> 0.08 us  [the longest x2 0.04 us: apart(): kept = jnp.stack([blocks[:, 0, :, 0], blocks[:, 1, :, 1]], axis=1)]
    pallas_call x0 -> x1, Pallas kernels: none -> 128 us  [delta_mix(): pl.pallas_call(delta_kernel, grid=(rows // BLOCK,), in_specs=[pl.BlockSpe...]
    dot_general x177 -> x1, matrix products: 108 us -> 2.06 us  [on_device(): jnp.einsum('tgj,gvj->tgv', map_reads.reshape(sequence_rows, groups, lanes...]
    all_gather x1, waiting for transfers between devices: 0.02 us -> 49.2 us  [on_device(): lax.all_gather(convolution_output, ('sp', 'fs'), axis=1, tiled=True)]
    all_gather x8 -> x2, waiting for transfers between devices: 268 us -> 222 us  [the longest x1 124 us: on_device(): lax.all_gather(state_weights, ('sp', 'fs'), axis=0, tiled=True)]
    mul x17 -> x1, other arithmetic: 28 us -> 0.3 us  [conv_branch(): product = pre_values.astype(jnp.float32) * conv_values.astype(jnp.float32)]
    dynamic_slice x32 -> x0, local copies, waits for them, and re-layouts: 16.4 us -> none  [on_device(): lax.scan(block_pass, initial_rows, tuple((in_blocks(array) for array in (...]
    dynamic_update_slice x16 -> x0, local copies, waits for them, and re-layouts: 13.9 us -> none  [on_device(): lax.scan(block_pass, initial_rows, tuple((in_blocks(array) for array in (...]
  transfers between devices with their start and end apart: 16 -> 10, of which waited for: 10 -> 8; matrix products, arithmetic and copies ran while one was open for 73% -> 8% of each run, Pallas kernels for 0% -> 25%
where the time goes in v1:
time: 523 us; the launch traced here: 522 us
  waiting for transfers between devices  305 us (58%)
  Pallas kernels  128 us (24%)
  matrix products  46.2 us (9%)
  starting transfers between devices  14.2 us (3%)
  between operations  13.9 us (3%)
  local copies, waits for them, and re-layouts  7.99 us (2%)
  other arithmetic  6.17 us (1%)
    pallas_call x1, Pallas kernels, delta_mix(): pl.pallas_call(delta_kernel, grid=(rows // BLOCK,), in_specs=[pl.BlockSpe...  128 us
    all_gather x1, waiting for transfers between devices, on_device(): lax.all_gather(state_weights, ('sp', 'fs'), axis=0, tiled=True)  124 us
    all_gather x1, waiting for transfers between devices, on_device(): lax.all_gather(conv_weights, ('sp', 'fs'), axis=0, tiled=True)  97.4 us
    all_gather x1, waiting for transfers between devices, on_device(): lax.all_gather(convolution_output, ('sp', 'fs'), axis=1, tiled=True)  49.2 us
    dot_general x2, matrix products, project(): jnp.dot(activations, weight, preferred_element_type=jnp.float32)  26.7 us
    ppermute x4, starting transfers between devices, passed_along(): return lax.ppermute(block, axis, route)  14 us
    reduce_scatter x1, waiting for transfers between devices, on_device(): lax.psum_scatter((jnp.dot(conv_mixed, conv_whole, preferred_element_type=...  13 us
    all_gather x1, waiting for transfers between devices, on_device(): piece = lax.all_gather(normed, 'tp', axis=0, tiled=True)  12.4 us
  transfers between devices with their start and end apart: 10, of which 8 were waited for; matrix products, arithmetic and copies ran while one was open for 8% of the time, Pallas kernels for 25%

profile of v1, /device:TPU:0, one launch (start us, length us, event | category | flops | bytes accessed | tf_op | source)
XLA Modules:
  0.0 522.3 jit_solution(5617639318536283837)
XLA Ops:
  6.5 2.2 fusion.5
  8.8 0.0 copy-done.1
  8.8 1.9 fusion.7
  10.7 0.0 copy-start.7
  10.7 0.0 copy-start.8
  10.7 0.0 copy-start.9
  10.7 0.0 copy-start.10
  10.7 0.0 all-gather.6.cloned.1.call-update
  10.7 0.0 all-gather.8.cloned.1.call-start
  10.8 0.8 copy-done.11
  11.6 0.1 copy-done.12
  11.6 0.1 copy-done.13
  11.7 0.8 pad_maximum_fusion.1
  12.5 0.0 all-gather.8.cloned.1.call-update
  12.5 0.0 all-gather.10.cloned.1.call-start
  12.5 0.7 all-gather.10.cloned.1.call-update
  13.2 0.0 all-gather.12.cloned.1.call-start
  13.3 0.0 copy-done.6
  13.4 0.8 copy-done.5
  14.3 0.0 all-gather.12.cloned.1.call-update
  14.3 0.0 all-gather.14.cloned.1.call-start
  14.3 0.5 all-gather.14.cloned.1.call-update
  14.9 0.0 reduce-scatter.2.cloned.1.call-start
  14.9 12.4 %all-gather.6.cloned.1.call-done = bf16[1024,2048]{1,0:T(8,128)(2,1)} async-done(((bf16[512,2048]{1,0:T(8,128)(2,1)}), bf16[1024,2048]{1,0:T(8,128)(2,1)}) %all-gather.6.cloned.1.call-update) | async-done | bytes 4194320 | tf_op jit(solution)/shard_map/all_gather | solution.py:265
  27.3 97.4 %all-gather.8.cloned.1.call-done = bf16[2048,1536]{1,0:T(8,128)(2,1)} async-done(((bf16[128,1536]{1,0:T(8,128)(2,1)}), bf16[2048,1536]{1,0:T(8,128)(2,1)}) %all-gather.8.cloned.1.call-update) | async-done | bytes 6291472 | tf_op jit(solution)/shard_map/all_gather | solution.py:271
  124.7 10.0 %convolution_convert_fusion.1 = bf16[1024,1536]{1,0:T(8,128)(2,1)S(1)} fusion(bf16[1024,2048]{1,0:T(8,128)(2,1)} %all-gather.6.cloned.1.call-done, bf16[2048,1536]{1,0:T(8,128)(2,1)} %all-gather.8.cloned.1.call-done), kind=kOutput, calls=%fused_computation.14 | convolution fusion | flops 6444023808 | bytes 13631488 | tf_op jit(solution)/shard_map/dot_general | solution.py:30
  134.7 0.0 copy-start.15
  134.7 0.3 convert_multiply_fusion.2
  135.0 1.4 copy-done.3
  136.4 3.3 collective-permute-start.1
  139.7 49.2 %all-gather.10.cloned.1.call-done = bf16[512,2048]{1,0:T(8,128)(2,1)} async-done(((bf16[512,128]{1,0:T(8,128)(2,1)}), bf16[512,2048]{1,0:T(8,128)(2,1)}) %all-gather.10.cloned.1.call-update) | async-done | bytes 2097168 | tf_op jit(solution)/shard_map/all_gather | solution.py:305
  188.9 0.0 collective-permute-done.1
  188.9 7.8 %fusion.17 = f32[1024,2048]{1,0:T(8,128)} fusion(bf16[512,2048]{1,0:T(8,128)(2,1)} %all-gather.10.cloned.1.call-done, f32[2,512]{1,0:T(2,128)S(1)} %collective-permute-done.1, f32[1024,512]{1,0:T(8,128)S(1)} %convert_multiply_fusion.2, bf16[1024,1536]{1,0:T(8,128)(2,1)} %copy-done.3, f32[512]{0:T(512)S(1)} %bitcast.78, f32[512]{0:T(512)S(1)} %bitcast.79, ...), kind=kOutput, calls=%fused_computation.32 | convolution fusion | flops 2152726528 | bytes 13641728 | tf_op jit(solution)/shard_map/dot_general | solution.py:310
  196.7 124.4 %all-gather.12.cloned.1.call-done = bf16[2048,2560]{1,0:T(8,128)(2,1)} async-done(((bf16[128,2560]{1,0:T(8,128)(2,1)}), bf16[2048,2560]{1,0:T(8,128)(2,1)}) %all-gather.12.cloned.1.call-update) | async-done | bytes 10485776 | tf_op jit(solution)/shard_map/all_gather | solution.py:266
  321.1 16.7 %convolution_convert_fusion.proj_ref = bf16[1024,2560]{1,0:T(8,128)(2,1)} fusion(bf16[1024,2048]{1,0:T(8,128)(2,1)} %all-gather.6.cloned.1.call-done, bf16[2048,2560]{1,0:T(8,128)(2,1)} %all-gather.12.cloned.1.call-done), kind=kOutput, calls=%fused_computation.8 | convolution fusion | flops 10740039680 | bytes 19922944 | tf_op jit(solution)/shard_map/dot_general | solution.py:30
  337.8 128.5 %shard_map.172 = (f32[1024,512]{1,0:T(8,128)}, bf16[1024,512]{1,0:T(8,128)(2,1)}, f32[4,256,128]{2,1,0:T(8,128)}) custom-call(bf16[1024,2560]{1,0:T(8,128)(2,1)} %convolution_convert_fusion.proj_ref, f32[1024,512]{1,0:T(8,128)} %bitcast.80, f32[1,512]{1,0:T(1,128)} %bitcast.81, f32[1,512]{1,0:T(1,128)} %bitcast.82), custom_call_target="tpu_custom_call" | custom-call | flops 2684354560 | bytes 10485760 | tf_op jit(solution)/shard_map/pallas_call | solution.py:193
  466.3 1.1 fusion.39
  467.3 0.3 reshape.65
  467.7 0.0 copy-start.2
  467.7 0.2 fusion.40
  468.0 0.3 reshape.67
  468.3 0.2 fusion.38
  468.6 0.6 copy-done.2
  469.3 1.8 copy.33
  471.1 19.8 %while.11 = (s32[]{:T(128)}, f32[8,64,64]{2,1,0:T(8,128)S(1)}, pred[]{:T(512)}, f32[8,64,64]{2,1,0:T(8,128)S(1)}, f32[8,64,64]{2,1,0:T(8,128)S(1)}, /*index=5*/f32[8,64,64]{2,1,0:T(8,128)S(1)}, s32[]{:T(128)}, s32[]{:T(128)}) while((s32[]{:T(128)}, f32[8,64,64]{2,1,0:T(8,128)S(1)}, pred[]{:T(512)}, f32[8,64,64]{2,1,0:T(8,128)S(1)}, ...), condition=%wide.region_2.3_spmd.clone, body=%wide.region_1.2_spmd.clone.sunk | while | flops 25329668 | bytes 1048712 | solution.py:286
  471.1 0.4 fusion.54
  471.5 2.0 collective-permute-start
  473.5 2.5 collective-permute-done
  476.0 0.4 fusion.54
  476.5 4.4 collective-permute-start
  480.8 2.5 collective-permute-done
  483.4 0.4 fusion.54
  483.8 4.4 collective-permute-start
  488.1 2.5 collective-permute-done
  490.9 2.1 bitcast_add_fusion
  493.0 0.0 copy-start.16
  493.0 0.2 reduce_sum.28
  493.3 0.3 multiply_reduce_fusion
  493.6 0.1 copy-done.16
  493.7 0.3 fusion.16
  494.0 0.0 all-gather.14.cloned.1.call-done
  494.0 8.5 %add_convert_fusion = bf16[1024,2048]{1,0:T(8,128)(2,1)} fusion(f32[1024,2048]{1,0:T(8,128)} %fusion.17, bf16[1024,512]{0,1:T(8,128)(2,1)S(1)} %fusion.16, bf16[512,2048]{1,0:T(8,128)(2,1)} %all-gather.14.cloned.1.call-done), kind=kOutput, calls=%fused_computation.7 | convolution fusion | flops 2151677952 | bytes 15728640 | tf_op jit(solution)/shard_map/dot_general | solution.py:311
  502.5 0.0 reduce-scatter.2.cloned.1.call-update
  502.5 13.0 %reduce-scatter.2.cloned.1.call-done = bf16[512,2048]{1,0:T(8,128)(2,1)} async-done(((bf16[1024,2048]{1,0:T(8,128)(2,1)}), bf16[512,2048]{1,0:T(8,128)(2,1)}) %reduce-scatter.2.cloned.1.call-update) | async-done | bytes 2097168 | tf_op jit(solution)/shard_map/reduce_scatter | solution.py:308
  (39 shorter events, 0.3 us)
Async XLA Ops:
  6.5 2.2 copy-start.1
  6.5 2.2 copy-start.14
  6.5 20.7 %all-gather.6.cloned.1.call-start = ((), (), s32[]{:S(2)}) async-start(), calls=%async_computation.1 | async-start | bytes 6291456 | tf_op jit(solution)/shard_map/all_gather | solution.py:265
  10.7 0.9 copy-start.11
  10.7 1.0 copy-start.12
  10.7 1.0 copy-start.13
  10.7 2.6 copy-start.6
  10.7 2.6 copy-start.7
  10.7 2.7 copy-start.8
  10.7 2.7 copy-start.9
  10.7 2.7 copy-start.10
  10.7 113.9 %all-gather.8.cloned.1.call-start = ((), (), s32[]{:S(2)}) async-start(), calls=%async_computation.2 | async-start | bytes 6684672 | tf_op jit(solution)/shard_map/all_gather | solution.py:271
  12.5 176.4 %all-gather.10.cloned.1.call-start = ((), (), s32[]{:S(2)}) async-start(), calls=%async_computation.3 | async-start | bytes 2228224 | tf_op jit(solution)/shard_map/all_gather | solution.py:305
  13.2 307.9 %all-gather.12.cloned.1.call-start = ((), (), s32[]{:S(2)}) async-start(), calls=%async_computation.4 | async-start | bytes 11141120 | tf_op jit(solution)/shard_map/all_gather | solution.py:266
  13.4 0.8 copy-start.5
  14.3 479.7 %all-gather.14.cloned.1.call-start = ((), (), s32[]{:S(2)}) async-start(), calls=%async_computation.5 | async-start | bytes 2228224 | tf_op jit(solution)/shard_map/all_gather | solution.py:306
  14.9 500.6 %reduce-scatter.2.cloned.1.call-start = ((), (), s32[]{:S(2)}) async-start(), calls=%async_computation.6 | async-start | bytes 6291456 | tf_op jit(solution)/shard_map/reduce_scatter | solution.py:308
  134.7 1.7 copy-start.3
  134.7 5.0 copy-start.15
  136.4 52.5 %collective-permute-start.1 = (f32[2,512]{1,0:T(2,128)S(1)}, f32[2,512]{1,0:T(2,128)S(1)}, u32[]{:S(2)}, u32[]{:S(2)}) collective-permute-start(f32[2,512]{1,0:T(2,128)S(1)} %slice.58), channel_id=1, source_target_pairs={{0,8},{8,16},{16,24},{1,9},{9,17},{17,25},{2,10},{10,18},{18,26},{... | collective-permute-start | bytes 12296 | tf_op jit(solution)/shard_map/ppermute | solution.py:20
  467.7 1.6 copy-start.2
  469.3 1.8 copy-start
  471.1 19.9 %copy-start.4 = (bf16[1024,512]{1,0:T(8,128)(2,1)S(1)}, bf16[1024,512]{1,0:T(8,128)(2,1)}, u32[]{:S(2)}) copy-start(bf16[1024,512]{1,0:T(8,128)(2,1)} %get-tuple-element.43) | copy-start | bytes 3145732
  471.5 4.5 collective-permute-start
  476.5 6.9 %collective-permute-start = (bf16[8,64,64]{2,1,0:T(8,128)(2,1)S(1)}, bf16[8,64,64]{2,1,0:T(8,128)(2,1)S(1)}, u32[]{:S(2)}, u32[]{:S(2)}) collective-permute-start(bf16[8,64,64]{2,1,0:T(8,128)(2,1)S(1)} %fusion.54), channel_id=1, source_target_pairs={{0,8},{8,16},{16,24},{1,9},{9,17},{17,25},{2,10},{10,18},{18,26},{... | collective-permute-start | bytes 196616 | tf_op jit(solution)/shard_map/while/body/eval_jaxpr/ppermute | solution.py:20
  483.8 6.9 %collective-permute-start = (bf16[8,64,64]{2,1,0:T(8,128)(2,1)S(1)}, bf16[8,64,64]{2,1,0:T(8,128)(2,1)S(1)}, u32[]{:S(2)}, u32[]{:S(2)}) collective-permute-start(bf16[8,64,64]{2,1,0:T(8,128)(2,1)S(1)} %fusion.54), channel_id=1, source_target_pairs={{0,8},{8,16},{16,24},{1,9},{9,17},{17,25},{2,10},{10,18},{18,26},{... | collective-permute-start | bytes 196616 | tf_op jit(solution)/shard_map/while/body/eval_jaxpr/ppermute | solution.py:20
  493.0 0.7 copy-start.16
Sparse Core Ops, SparseCore 0:
  10.9 16.3 all-gather.5
  30.1 94.5 all-gather.7
  127.4 61.4 all-gather.9
  191.4 129.6 all-gather.11
  323.7 62.2 all-gather.13
  502.6 12.7 reduce-scatter.1

commit v2 on v1

--- a/solution.py
+++ b/solution.py
@@ -7,6 +7,7 @@
 
 HEAD_WIDTH = 64
 BLOCK = 64
+STEP_BLOCKS = 2
 
 
 norm_eps = 1e-06
@@ -69,19 +70,25 @@
     return total
 
 
-def unit_inverse(lower, row, col, size):
-    inverse = jnp.where(row == col, 1.0, 0.0) - jnp.where(
-        ((row ^ col) == 1) & (row > col), lower, 0.0
-    )
+def unit_inverses(lowers, row, col, size):
+    odd = ((row ^ col) == 1) & (row > col)
+    eye = jnp.where(row == col, 1.0, 0.0)
+    inverses = [eye - jnp.where(odd, lower, 0.0) for lower in lowers]
+    lowers = [lower.astype(jnp.bfloat16) for lower in lowers]
     width = 2
     while width < size:
         cross = ((row // (2 * width)) == (col // (2 * width))) & (
             (row // width) > (col // width)
         )
-        step = dot_bf16(jnp.where(cross, lower, 0.0), inverse, ROWS)
-        inverse = inverse - dot_bf16(inverse, step, ROWS)
+        nears = [inverse.astype(jnp.bfloat16) for inverse in inverses]
+        steps = [
+            dot_bf16(jnp.where(cross, lower, jnp.zeros_like(lower)), near, ROWS)
+            for lower, near in zip(lowers, nears)
+        ]
+        turns = [dot_bf16(near, step, ROWS) for near, step in zip(nears, steps)]
+        inverses = [inverse - turn for inverse, turn in zip(inverses, turns)]
         width *= 2
-    return inverse
+    return inverses
 
 
 def delta_kernel(proj_ref, spike_ref, floor_ref, offset_ref, reads_ref, maps_ref, ending_ref, state):
@@ -99,86 +106,119 @@
         for group in range(groups):
             state[group] = start
 
-    def part(index):
-        return proj_ref[:, index * channels : (index + 1) * channels].astype(jnp.float32)
-
-    queries, keys, values, decay_pre, rate_pre = [part(i) for i in range(5)]
-    log_decay = -jnp.exp(floor_ref[...] + jnp.tanh(decay_pre)) + spike_ref[...]
-    rate = jax.nn.sigmoid(offset_ref[...] + rate_pre)
-    tri = lax.broadcasted_iota(jnp.int32, (span, span), 0) >= lax.broadcasted_iota(
-        jnp.int32, (span, span), 1
-    )
-    cumulative = split_dot(jnp.where(tri, 1.0, 0.0), log_decay, ROWS, True)
-    previous = cumulative - log_decay
-    middle = cumulative[span // 2 : span // 2 + 1]
-    closing = cumulative[span - 1 : span]
+    spans = [slice(at, at + BLOCK) for at in range(0, span, BLOCK)]
+    tri = lax.broadcasted_iota(jnp.int32, (BLOCK, BLOCK), 0) >= lax.broadcasted_iota(
+        jnp.int32, (BLOCK, BLOCK), 1
+    )
+    tri = jnp.where(tri, 1.0, 0.0)
     square = lax.broadcasted_iota(jnp.int32, (lanes, lanes), 0)
     across = lax.broadcasted_iota(jnp.int32, (lanes, lanes), 1)
     same_head = jnp.where((square // HEAD_WIDTH) == (across // HEAD_WIDTH), 1.0, 0.0)
-    first_lanes = lax.broadcasted_iota(jnp.int32, (span, lanes), 1) < HEAD_WIDTH
-
-    def by_head(array):
-        return jnp.concatenate(
-            [jnp.where(first_lanes, array, 0.0), jnp.where(first_lanes, 0.0, array)], axis=0
-        ).astype(jnp.bfloat16)
-
-    grow = jnp.exp(middle - cumulative)
-    shrink_previous = jnp.exp(previous - middle)
-    shrink = jnp.exp(cumulative - middle)
-    from_previous = jnp.exp(previous)
-    from_current = jnp.exp(cumulative)
-    tail = jnp.exp(closing - cumulative)
-    whole = jnp.exp(closing)
+    first_lanes = lax.broadcasted_iota(jnp.int32, (BLOCK, lanes), 1) < HEAD_WIDTH
     strict = square > across
     inclusive = square >= across
-    for group in range(groups):
-        cols = slice(group * lanes, (group + 1) * lanes)
-        key = keys[:, cols]
-        query = queries[:, cols]
-        square_sum = split_dot(same_head, key * key, ROWS, False)
-        unit = key * lax.rsqrt(square_sum + key_eps)
-        beta = rate[:, cols] * unit
-        value = by_head(values[:, cols])
-        asks = jnp.concatenate(
-            [by_head(unit * shrink_previous[:, cols]), by_head(query * shrink[:, cols])], axis=0
+
+    def by_head(array):
+        array = array.astype(jnp.bfloat16)
+        zeros = jnp.zeros_like(array)
+        return jnp.concatenate(
+            [jnp.where(first_lanes, array, zeros), jnp.where(first_lanes, zeros, array)], axis=0
         )
-        gives = jnp.concatenate(
-            [by_head(key * grow[:, cols]), by_head(beta * grow[:, cols])], axis=0
+
+    def stacked(*arrays):
+        return jnp.concatenate([by_head(array) for array in arrays], axis=0)
+
+    work = [(at, group) for at in spans for group in range(groups)]
+
+    def part(index, at, group):
+        begin = index * channels + group * lanes
+        return proj_ref[at, begin : begin + lanes].astype(jnp.float32)
+
+    def column(ref, at, group):
+        return ref[at, group * lanes : (group + 1) * lanes]
+
+    asks, gives, openers, tails, values, wholes = [], [], [], [], [], []
+    every = slice(0, 1)
+    logs = [
+        -jnp.exp(column(floor_ref, every, g) + jnp.tanh(part(3, at, g))) + column(spike_ref, at, g)
+        for at, g in work
+    ]
+    sums = [split_dot(tri, log, ROWS, True) for log in logs]
+    raw_keys = [part(1, at, g) for at, g in work]
+    norms = [split_dot(same_head, key * key, ROWS, False) for key in raw_keys]
+    for (at, g), log, cumulative, key, norm in zip(work, logs, sums, raw_keys, norms):
+        query = part(0, at, g)
+        unit = key * lax.rsqrt(norm + key_eps)
+        beta = jax.nn.sigmoid(column(offset_ref, every, g) + part(4, at, g)) * unit
+        previous = cumulative - log
+        middle = cumulative[BLOCK // 2 : BLOCK // 2 + 1]
+        closing = cumulative[BLOCK - 1 : BLOCK]
+        grow = jnp.exp(middle - cumulative)
+        tail = jnp.exp(closing - cumulative)
+        asks.append(stacked(unit * jnp.exp(previous - middle), query * jnp.exp(cumulative - middle)))
+        gives.append(stacked(key * grow, beta * grow))
+        openers.append(stacked(unit * jnp.exp(previous), query * jnp.exp(cumulative)))
+        tails.append(stacked(key * tail, beta * tail))
+        values.append(by_head(part(2, at, g)))
+        wholes.append(jnp.exp(closing))
+    grams = [dot_bf16(ask, give, TRANSPOSED_RIGHT) for ask, give in zip(asks, gives)]
+    inners = [
+        dot_bf16(
+            jnp.concatenate(
+                [
+                    jnp.where(strict, gram[:lanes, :lanes], 0.0),
+                    jnp.where(inclusive, gram[lanes:, :lanes], 0.0),
+                ],
+                axis=0,
+            ),
+            value,
+            ROWS,
         )
-        grams = dot_bf16(asks, gives, TRANSPOSED_RIGHT)
-        key_ask = jnp.where(strict, grams[:lanes, :lanes], 0.0)
-        beta_ask = jnp.where(strict, grams[:lanes, lanes:], 0.0)
-        key_read = jnp.where(inclusive, grams[lanes:, :lanes], 0.0)
-        beta_read = jnp.where(inclusive, grams[lanes:, lanes:], 0.0)
-        inverse = unit_inverse(beta_ask, square, across, span)
-        carried = state[group]
-        openers = jnp.concatenate(
-            [by_head(unit * from_previous[:, cols]), by_head(query * from_current[:, cols])],
-            axis=0,
-        )
-        opened = dot_bf16(openers, carried, TRANSPOSED_RIGHT)
-        inner = dot_bf16(jnp.concatenate([key_ask, key_read], axis=0), value, ROWS)
-        right_side = jnp.concatenate(
-            [opened[:lanes, :lanes] + inner[:lanes], opened[:lanes, lanes:]], axis=1
-        )
-        removed = dot_bf16(inverse, right_side, ROWS)
-        taken = dot_bf16(beta_read, removed, ROWS)
-        out_source = opened[lanes:, :lanes] + inner[lanes:] - taken[:, :lanes]
-        out_map = opened[lanes:, lanes:] - taken[:, lanes:]
-        reads_ref[:, cols] = out_source[:span] + out_source[span:]
-        maps_ref[:, cols] = (out_map[:span] + out_map[span:]).astype(maps_ref.dtype)
-        tails = jnp.concatenate(
-            [by_head(key * tail[:, cols]), by_head(beta * tail[:, cols])], axis=0
-        )
-        lefts = jnp.concatenate(
-            [
-                jnp.concatenate([value, jnp.zeros_like(value)], axis=1),
-                (-removed).astype(jnp.bfloat16),
-            ],
-            axis=0,
-        )
-        carried = carried * whole[:, cols] + dot_bf16(lefts, tails, TRANSPOSED_LEFT)
-        state[group] = carried
+        for gram, value in zip(grams, values)
+    ]
+    beta_reads = [
+        jnp.where(inclusive, gram[lanes:, lanes:], 0.0).astype(jnp.bfloat16) for gram in grams
+    ]
+    inverses = unit_inverses(
+        [jnp.where(strict, gram[:lanes, lanes:], 0.0) for gram in grams], square, across, BLOCK
+    )
+    inverses = [inverse.astype(jnp.bfloat16) for inverse in inverses]
+    for index, at in enumerate(spans):
+        picks = range(index * groups, (index + 1) * groups)
+        carried = [state[g] for g in range(groups)]
+        opened = [dot_bf16(openers[i], carried[g], TRANSPOSED_RIGHT) for g, i in enumerate(picks)]
+        rights = [
+            jnp.concatenate(
+                [opened[g][:lanes, :lanes] + inners[i][:lanes], opened[g][:lanes, lanes:]], axis=1
+            )
+            for g, i in enumerate(picks)
+        ]
+        removed = [
+            dot_bf16(inverses[i], rights[g], ROWS).astype(jnp.bfloat16)
+            for g, i in enumerate(picks)
+        ]
+        changes = [
+            dot_bf16(
+                jnp.concatenate(
+                    [
+                        jnp.concatenate([values[i], jnp.zeros_like(values[i])], axis=1),
+                        -removed[g],
+                    ],
+                    axis=0,
+                ),
+                tails[i],
+                TRANSPOSED_LEFT,
+            )
+            for g, i in enumerate(picks)
+        ]
+        taken = [dot_bf16(beta_reads[i], removed[g], ROWS) for g, i in enumerate(picks)]
+        for g, i in enumerate(picks):
+            state[g] = carried[g] * wholes[i] + changes[g]
+            cols = slice(g * lanes, (g + 1) * lanes)
+            out_source = opened[g][lanes:, :lanes] + inners[i][lanes:] - taken[g][:, :lanes]
+            out_map = opened[g][lanes:, lanes:] - taken[g][:, lanes:]
+            reads_ref[at, cols] = out_source[:BLOCK] + out_source[BLOCK:]
+            maps_ref[at, cols] = (out_map[:BLOCK] + out_map[BLOCK:]).astype(maps_ref.dtype)
 
     @pl.when(chunk == pl.num_programs(0) - 1)
     def _():
@@ -190,18 +230,19 @@
     lanes = 2 * HEAD_WIDTH
     groups = channels // lanes
     wide = projected.shape[1]
+    turn = STEP_BLOCKS * BLOCK
     return pl.pallas_call(
         delta_kernel,
-        grid=(rows // BLOCK,),
+        grid=(rows // turn,),
         in_specs=[
-            pl.BlockSpec((BLOCK, wide), lambda i: (i, 0)),
-            pl.BlockSpec((BLOCK, channels), lambda i: (i, 0)),
+            pl.BlockSpec((turn, wide), lambda i: (i, 0)),
+            pl.BlockSpec((turn, channels), lambda i: (i, 0)),
             pl.BlockSpec((1, channels), lambda i: (0, 0)),
             pl.BlockSpec((1, channels), lambda i: (0, 0)),
         ],
         out_specs=[
-            pl.BlockSpec((BLOCK, channels), lambda i: (i, 0)),
-            pl.BlockSpec((BLOCK, channels), lambda i: (i, 0)),
+            pl.BlockSpec((turn, channels), lambda i: (i, 0)),
+            pl.BlockSpec((turn, channels), lambda i: (i, 0)),
             pl.BlockSpec((groups, 2 * lanes, lanes), lambda i: (0, 0, 0)),
         ],
         out_shape=[
@@ -263,7 +304,12 @@
     )
     conv_weights = jnp.concatenate([earlier_gate, later_gate, convolution_input], axis=1)
     piece = lax.all_gather(normed, "tp", axis=0, tiled=True)
-    projected = project(piece, lax.all_gather(state_weights, ("sp", "fs"), axis=0, tiled=True))
+    state_whole = lax.all_gather(state_weights, ("sp", "fs"), axis=0, tiled=True)
+    outgoing = jnp.concatenate([convolution_output, state_heads_output], axis=0)
+    state_whole, conv_weights, outgoing = lax.optimization_barrier(
+        (state_whole, conv_weights, outgoing)
+    )
+    projected = project(piece, state_whole)
     sequence_rows = projected.shape[0]
     present_heads = channels // HEAD_WIDTH
     source_reads, map_reads, ending = delta_mix(projected, decay_spike[0], decay_floor, rate_offset)
@@ -301,14 +347,14 @@
         * head_norm_gain.reshape(present_heads, HEAD_WIDTH)
     )
     state_mixed = state_mixed.reshape(sequence_rows, channels).astype(jnp.bfloat16)
-    conv_whole, state_whole = (
-        lax.all_gather(convolution_output, ("sp", "fs"), axis=1, tiled=True),
-        lax.all_gather(state_heads_output, ("sp", "fs"), axis=1, tiled=True),
-    )
+    out_whole = lax.all_gather(outgoing, ("sp", "fs"), axis=1, tiled=True)
     mixed = lax.psum_scatter(
         (
-            jnp.dot(conv_mixed, conv_whole, preferred_element_type=jnp.float32)
-            + jnp.dot(state_mixed, state_whole, preferred_element_type=jnp.float32)
+            jnp.dot(
+                jnp.concatenate([conv_mixed, state_mixed], axis=1),
+                out_whole,
+                preferred_element_type=jnp.float32,
+            )
         ).astype(jnp.bfloat16),
         "tp",
         scatter_dimension=0,

time: 523 us -> 379 us (0.72)
  Pallas kernels: 128 us -> 31.7 us
  waiting for transfers between devices: 305 us -> 239 us
  local copies, waits for them, and re-layouts: 7.99 us -> 21.9 us
  starting transfers between devices: 14.2 us -> 26 us
  matrix products: 46.2 us -> 38.1 us
    all_gather x1, waiting for transfers between devices: 97.4 us -> 0.01 us  [on_device(): lax.all_gather(conv_weights, ('sp', 'fs'), axis=0, tiled=True)]
    pallas_call x1, Pallas kernels: 128 us -> 31.7 us  [delta_mix(): pl.pallas_call(delta_kernel, grid=(rows // turn,), in_specs=[pl.BlockSpec...]
    all_gather x2 -> x1, waiting for transfers between devices: 49.2 us -> 70.3 us  [on_device(): out_whole = lax.all_gather(outgoing, ('sp', 'fs'), axis=1, tiled=True)]
    ppermute x4, starting transfers between devices: 14 us -> 25.8 us  [passed_along(): return lax.ppermute(block, axis, route)]
    ppermute x4, waiting for transfers between devices: 7.49 us -> 17.3 us  [passed_along(): return lax.ppermute(block, axis, route)]
    dot_general x2 -> x1, matrix products: 16.3 us -> 8.18 us  [on_device(): jnp.dot(jnp.concatenate([conv_mixed, state_mixed], axis=1), out_whole, pr...]
  transfers between devices with their start and end apart: 10 -> 9, of which waited for: 8 -> 8; matrix products, arithmetic and copies ran while one was open for 8% -> 14% of each run, Pallas kernels for 25% -> 8%
where the time goes in v2:
time: 379 us
  waiting for transfers between devices  239 us (63%)
  matrix products  38.1 us (10%)
  Pallas kernels  31.7 us (8%)
  starting transfers between devices  26 us (7%)
  local copies, waits for them, and re-layouts  21.9 us (6%)
  between operations  13.5 us (4%)
  other arithmetic  8.07 us (2%)
    all_gather x1, waiting for transfers between devices, on_device(): lax.all_gather(state_weights, ('sp', 'fs'), axis=0, tiled=True)  128 us
    all_gather x1, waiting for transfers between devices, on_device(): out_whole = lax.all_gather(outgoing, ('sp', 'fs'), axis=1, tiled=True)  70.3 us
    pallas_call x1, Pallas kernels, delta_mix(): pl.pallas_call(delta_kernel, grid=(rows // turn,), in_specs=[pl.BlockSpec...  31.7 us
    dot_general x2, matrix products, project(): jnp.dot(activations, weight, preferred_element_type=jnp.float32)  26.7 us
    ppermute x4, starting transfers between devices, passed_along(): return lax.ppermute(block, axis, route)  25.8 us
    ppermute x4, waiting for transfers between devices, passed_along(): return lax.ppermute(block, axis, route)  17.3 us
    all_gather x1, waiting for transfers between devices, on_device(): piece = lax.all_gather(normed, 'tp', axis=0, tiled=True)  12.8 us
    reduce_scatter x1, waiting for transfers between devices, on_device(): lax.psum_scatter(jnp.dot(jnp.concatenate([conv_mixed, state_mixed], axis=...  10.4 us
  transfers between devices with their start and end apart: 9, of which 8 were waited for; matrix products, arithmetic and copies ran while one was open for 14% of the time, Pallas kernels for 8%

profile of v2, /device:TPU:0, one launch (start us, length us, event | category | flops | bytes accessed | tf_op | source)
XLA Modules:
  0.0 378.5 jit_solution(12154205806679699728)
XLA Ops:
  6.5 0.0 all-gather.7.cloned.1.call-start
  6.5 1.1 constant_dynamic-update-slice_fusion.4
  7.6 0.9 constant_dynamic-update-slice_fusion.3
  8.5 0.9 constant_dynamic-update-slice_fusion.2
  9.4 0.9 constant_dynamic-update-slice_fusion.1
  10.4 0.9 constant_dynamic-update-slice_fusion
  11.3 0.8 copy-done.7
  12.1 0.0 all-gather.7.cloned.1.call-update
  12.2 0.0 all-gather.5.cloned.1.call-start
  12.2 2.1 fusion.5
  14.3 1.9 fusion.7
  16.2 0.0 copy-start.12
  16.2 0.0 copy-start.14
  16.2 0.0 all-gather.5.cloned.1.call-update
  16.2 0.0 all-gather.9.cloned.1.call-start
  16.3 0.8 copy-done.8
  17.1 0.1 copy-done.9
  17.1 0.7 pad_maximum_fusion.2
  17.9 0.8 pad_maximum_fusion.1
  18.7 127.8 %all-gather.7.cloned.1.call-done = bf16[2048,2560]{1,0:T(8,128)(2,1)} async-done(((bf16[128,2560]{1,0:T(8,128)(2,1)}), bf16[2048,2560]{1,0:T(8,128)(2,1)}) %all-gather.7.cloned.1.call-update) | async-done | bytes 10485776 | tf_op jit(solution)/shard_map/all_gather | solution.py:307
  146.5 0.0 all-gather.9.cloned.1.call-update
  146.5 0.0 all-gather.11.cloned.1.call-start
  146.6 0.5 all-gather.11.cloned.1.call-update
  147.1 0.0 reduce-scatter.2.cloned.1.call-start
  147.1 12.8 %all-gather.5.cloned.1.call-done = bf16[1024,2048]{1,0:T(8,128)(2,1)} async-done(((bf16[512,2048]{1,0:T(8,128)(2,1)}), bf16[1024,2048]{1,0:T(8,128)(2,1)}) %all-gather.5.cloned.1.call-update) | async-done | bytes 4194320 | tf_op jit(solution)/shard_map/all_gather | solution.py:306
  159.9 16.5 %convolution_convert_fusion.proj_ref = bf16[1024,2560]{1,0:T(8,128)(2,1)} fusion(bf16[1024,2048]{1,0:T(8,128)(2,1)} %all-gather.5.cloned.1.call-done, bf16[2048,2560]{1,0:T(8,128)(2,1)} %all-gather.7.cloned.1.call-done), kind=kOutput, calls=%fused_computation.7 | convolution fusion | flops 10740039680 | bytes 19922944 | tf_op jit(solution)/shard_map/dot_general | solution.py:31
  176.4 31.7 %shard_map.172 = (f32[1024,512]{1,0:T(8,128)}, bf16[1024,512]{1,0:T(8,128)(2,1)}, f32[4,256,128]{2,1,0:T(8,128)}) custom-call(bf16[1024,2560]{1,0:T(8,128)(2,1)} %convolution_convert_fusion.proj_ref, f32[1024,512]{1,0:T(8,128)} %bitcast.72, f32[1,512]{1,0:T(1,128)} %bitcast.73, f32[1,512]{1,0:T(1,128)} %bitcast.74), custom_call_target="tpu_custom_call" | custom-call | flops 2684354560 | bytes 10485760 | tf_op jit(solution)/shard_map/pallas_call | solution.py:234
  208.1 1.1 fusion.34
  209.2 0.3 reshape.67
  209.5 0.0 copy-start.5
  209.5 0.2 fusion.33
  209.8 0.3 reshape.65
  210.2 0.2 fusion.35
  210.5 0.6 copy-done.5
  211.1 1.8 copy.38
  212.9 35.5 %while.11 = (s32[]{:T(128)}, f32[8,64,64]{2,1,0:T(8,128)S(1)}, pred[]{:T(512)}, f32[8,64,64]{2,1,0:T(8,128)S(1)}, f32[8,64,64]{2,1,0:T(8,128)S(1)}, /*index=5*/f32[8,64,64]{2,1,0:T(8,128)S(1)}, s32[]{:T(128)}, s32[]{:T(128)}) while((s32[]{:T(128)}, f32[8,64,64]{2,1,0:T(8,128)S(1)}, pred[]{:T(512)}, f32[8,64,64]{2,1,0:T(8,128)S(1)}, ...), condition=%wide.region_2.3_spmd.clone, body=%wide.region_1.2_spmd.clone.sunk | while | flops 25329668 | bytes 1048712 | solution.py:332
  212.9 0.4 fusion.47
  213.3 3.7 collective-permute-start
  217.0 6.0 %collective-permute-done = bf16[8,64,64]{2,1,0:T(8,128)(2,1)S(1)} collective-permute-done((bf16[8,64,64]{2,1,0:T(8,128)(2,1)S(1)}, bf16[8,64,64]{2,1,0:T(8,128)(2,1)S(1)}, u32[]{:S(2)}, u32[]{:S(2)}) %collective-permute-start) | collective-permute-done | bytes 65568 | tf_op jit(solution)/shard_map/while/body/eval_jaxpr/ppermute | solution.py:21
  223.1 0.4 fusion.47
  223.5 6.2 %collective-permute-start = (bf16[8,64,64]{2,1,0:T(8,128)(2,1)S(1)}, bf16[8,64,64]{2,1,0:T(8,128)(2,1)S(1)}, u32[]{:S(2)}, u32[]{:S(2)}) collective-permute-start(bf16[8,64,64]{2,1,0:T(8,128)(2,1)S(1)} %fusion.47), channel_id=1, source_target_pairs={{0,8},{8,16},{16,24},{1,9},{9,17},{17,25},{2,10},{10,18},{18,26},{... | collective-permute-start | bytes 196616 | tf_op jit(solution)/shard_map/while/body/eval_jaxpr/ppermute | solution.py:21
  229.7 5.5 %collective-permute-done = bf16[8,64,64]{2,1,0:T(8,128)(2,1)S(1)} collective-permute-done((bf16[8,64,64]{2,1,0:T(8,128)(2,1)S(1)}, bf16[8,64,64]{2,1,0:T(8,128)(2,1)S(1)}, u32[]{:S(2)}, u32[]{:S(2)}) %collective-permute-start) | collective-permute-done | bytes 65568 | tf_op jit(solution)/shard_map/while/body/eval_jaxpr/ppermute | solution.py:21
  235.2 0.4 fusion.47
  235.6 7.4 %collective-permute-start = (bf16[8,64,64]{2,1,0:T(8,128)(2,1)S(1)}, bf16[8,64,64]{2,1,0:T(8,128)(2,1)S(1)}, u32[]{:S(2)}, u32[]{:S(2)}) collective-permute-start(bf16[8,64,64]{2,1,0:T(8,128)(2,1)S(1)} %fusion.47), channel_id=1, source_target_pairs={{0,8},{8,16},{16,24},{1,9},{9,17},{17,25},{2,10},{10,18},{18,26},{... | collective-permute-start | bytes 196616 | tf_op jit(solution)/shard_map/while/body/eval_jaxpr/ppermute | solution.py:21
  243.1 5.4 %collective-permute-done = bf16[8,64,64]{2,1,0:T(8,128)(2,1)S(1)} collective-permute-done((bf16[8,64,64]{2,1,0:T(8,128)(2,1)S(1)}, bf16[8,64,64]{2,1,0:T(8,128)(2,1)S(1)}, u32[]{:S(2)}, u32[]{:S(2)}) %collective-permute-start) | collective-permute-done | bytes 65568 | tf_op jit(solution)/shard_map/while/body/eval_jaxpr/ppermute | solution.py:21
  248.6 2.1 bitcast_add_fusion
  250.6 0.2 reduce_sum.28
  250.9 0.3 multiply_reduce_fusion
  251.2 1.6 mul.95
  252.8 2.9 copy.37
  255.7 1.6 sub.13
  257.3 2.9 copy.36
  260.2 1.8 copy.39
  262.0 10.1 %convolution_convert_fusion.1 = bf16[1024,1536]{1,0:T(8,128)(2,1)S(1)} fusion(bf16[1024,2048]{1,0:T(8,128)(2,1)} %all-gather.5.cloned.1.call-done, bf16[2048,1536]{1,0:T(8,128)(2,1)} %all-gather.9.cloned.1.call-done), kind=kOutput, calls=%fused_computation.13 | convolution fusion | flops 6444023808 | bytes 13631488 | tf_op jit(solution)/shard_map/dot_general | solution.py:31
  272.1 0.0 copy-start.15
  272.1 0.3 convert_multiply_fusion.2
  272.5 8.5 %collective-permute-start.1 = (f32[2,512]{1,0:T(2,128)S(1)}, f32[2,512]{1,0:T(2,128)S(1)}, u32[]{:S(2)}, u32[]{:S(2)}) collective-permute-start(f32[2,512]{1,0:T(2,128)S(1)} %slice.58), channel_id=1, source_target_pairs={{0,8},{8,16},{16,24},{1,9},{9,17},{17,25},{2,10},{10,18},{18,26},{... | collective-permute-start | bytes 12296 | tf_op jit(solution)/shard_map/ppermute | solution.py:21
  281.1 0.8 multiply_convert_fusion
  281.9 0.4 collective-permute-done.1
  282.3 0.8 fusion.13
  283.1 70.3 %all-gather.11.cloned.1.call-done = bf16[1024,2048]{1,0:T(8,128)(2,1)} async-done(((bf16[1024,128]{1,0:T(8,128)(2,1)}), bf16[1024,2048]{1,0:T(8,128)(2,1)}) %all-gather.11.cloned.1.call-update) | async-done | bytes 4194320 | tf_op jit(solution)/shard_map/all_gather | solution.py:350
  353.4 8.2 %convolution_convert_fusion.2 = bf16[1024,2048]{1,0:T(8,128)(2,1)} fusion(bf16[1024,2048]{1,0:T(8,128)(2,1)} %all-gather.11.cloned.1.call-done, bf16[1024,512]{1,0:T(8,128)(2,1)S(1)} %multiply_convert_fusion, bf16[1024,512]{1,0:T(8,128)(2,1)S(1)} %fusion.13), kind=kOutput, calls=%fused_computation.14 | convolution fusion | flops 4301258752 | bytes 10485760 | tf_op jit(solution)/shard_map/dot_general | solution.py:353
  361.6 0.0 reduce-scatter.2.cloned.1.call-update
  361.6 10.4 %reduce-scatter.2.cloned.1.call-done = bf16[512,2048]{1,0:T(8,128)(2,1)} async-done(((bf16[1024,2048]{1,0:T(8,128)(2,1)}), bf16[512,2048]{1,0:T(8,128)(2,1)}) %reduce-scatter.2.cloned.1.call-update) | async-done | bytes 2097168 | tf_op jit(solution)/shard_map/reduce_scatter | solution.py:351
  (40 shorter events, 0.3 us)
Async XLA Ops:
  6.5 7.8 %copy-start.1 = (bf16[1,512,2048]{2,1,0:T(8,128)(2,1)S(1)}, bf16[1,512,2048]{2,1,0:T(8,128)(2,1)}, u32[]{:S(2)}) copy-start(bf16[1,512,2048]{2,1,0:T(8,128)(2,1)} %param.20) | copy-start | bytes 6291460
  6.5 7.8 %copy-start.13 = (f32[2048]{0:T(1024)S(1)}, f32[2048]{0:T(1024)}, u32[]{:S(2)}) copy-start(f32[2048]{0:T(1024)} %param.21) | copy-start | bytes 24580
  6.5 140.0 %all-gather.7.cloned.1.call-start = ((), (), s32[]{:S(2)}) async-start(), calls=%async_computation.2 | async-start | bytes 11141120 | tf_op jit(solution)/shard_map/all_gather | solution.py:307
  11.3 0.8 copy-start.7
  12.2 147.8 %all-gather.5.cloned.1.call-start = ((), (), s32[]{:S(2)}) async-start(), calls=%async_computation.1 | async-start | bytes 6291456 | tf_op jit(solution)/shard_map/all_gather | solution.py:306
  16.2 0.9 copy-start.8
  16.2 1.0 copy-start.9
  16.2 1.7 copy-start.10
  16.2 1.7 copy-start.11
  16.2 1.7 copy-start.12
  16.2 130.4 %copy-start.14 = (f32[3,512]{1,0:T(4,128)S(1)}, f32[3,512]{1,0:T(4,128)}, u32[]{:S(2)}) copy-start(f32[3,512]{1,0:T(4,128)} %param.25) | copy-start | bytes 18436
  16.2 245.7 %all-gather.9.cloned.1.call-start = ((), (), s32[]{:S(2)}) async-start(), calls=%async_computation.3 | async-start | bytes 6684672 | tf_op jit(solution)/shard_map/all_gather | solution.py:317
  146.5 206.9 %all-gather.11.cloned.1.call-start = ((), (), s32[]{:S(2)}) async-start(), calls=%async_computation.4 | async-start | bytes 4456448 | tf_op jit(solution)/shard_map/all_gather | solution.py:350
  147.1 224.9 %reduce-scatter.2.cloned.1.call-start = ((), (), s32[]{:S(2)}) async-start(), calls=%async_computation.5 | async-start | bytes 6291456 | tf_op jit(solution)/shard_map/reduce_scatter | solution.py:351
  209.5 1.6 copy-start.5
  211.1 1.8 copy-start
  212.9 35.6 %copy-start.6 = (bf16[1024,512]{1,0:T(8,128)(2,1)S(1)}, bf16[1024,512]{1,0:T(8,128)(2,1)}, u32[]{:S(2)}) copy-start(bf16[1024,512]{1,0:T(8,128)(2,1)} %get-tuple-element.48) | copy-start | bytes 3145732
  213.3 9.7 %collective-permute-start = (bf16[8,64,64]{2,1,0:T(8,128)(2,1)S(1)}, bf16[8,64,64]{2,1,0:T(8,128)(2,1)S(1)}, u32[]{:S(2)}, u32[]{:S(2)}) collective-permute-start(bf16[8,64,64]{2,1,0:T(8,128)(2,1)S(1)} %fusion.47), channel_id=1, source_target_pairs={{0,8},{8,16},{16,24},{1,9},{9,17},{17,25},{2,10},{10,18},{18,26},{... | collective-permute-start | bytes 196616 | tf_op jit(solution)/shard_map/while/body/eval_jaxpr/ppermute | solution.py:21
  223.5 11.7 %collective-permute-start = (bf16[8,64,64]{2,1,0:T(8,128)(2,1)S(1)}, bf16[8,64,64]{2,1,0:T(8,128)(2,1)S(1)}, u32[]{:S(2)}, u32[]{:S(2)}) collective-permute-start(bf16[8,64,64]{2,1,0:T(8,128)(2,1)S(1)} %fusion.47), channel_id=1, source_target_pairs={{0,8},{8,16},{16,24},{1,9},{9,17},{17,25},{2,10},{10,18},{18,26},{... | collective-permute-start | bytes 196616 | tf_op jit(solution)/shard_map/while/body/eval_jaxpr/ppermute | solution.py:21
  235.6 12.8 %collective-permute-start = (bf16[8,64,64]{2,1,0:T(8,128)(2,1)S(1)}, bf16[8,64,64]{2,1,0:T(8,128)(2,1)S(1)}, u32[]{:S(2)}, u32[]{:S(2)}) collective-permute-start(bf16[8,64,64]{2,1,0:T(8,128)(2,1)S(1)} %fusion.47), channel_id=1, source_target_pairs={{0,8},{8,16},{16,24},{1,9},{9,17},{17,25},{2,10},{10,18},{18,26},{... | collective-permute-start | bytes 196616 | tf_op jit(solution)/shard_map/while/body/eval_jaxpr/ppermute | solution.py:21
  262.0 19.1 %copy-start.4 = (f32[1024,512]{1,0:T(8,128)S(1)}, f32[1024,512]{1,0:T(8,128)}, u32[]{:S(2)}) copy-start(f32[1024,512]{1,0:T(8,128)} %copy.39) | copy-start | bytes 6291460
  272.1 8.9 %copy-start.2 = (f32[1024,512]{1,0:T(8,128)S(1)}, f32[1024,512]{1,0:T(8,128)}, u32[]{:S(2)}) copy-start(f32[1024,512]{1,0:T(8,128)} %copy.37) | copy-start | bytes 6291460
  272.1 8.9 %copy-start.3 = (f32[1024,512]{1,0:T(8,128)S(1)}, f32[1024,512]{1,0:T(8,128)}, u32[]{:S(2)}) copy-start(f32[1024,512]{1,0:T(8,128)} %copy.36) | copy-start | bytes 6291460
  272.1 8.9 %copy-start.15 = (f32[512]{0:T(512)S(1)}, f32[512]{0:T(512)}, u32[]{:S(2)}) copy-start(f32[512]{0:T(512)} %param.35) | copy-start | bytes 6148
  272.5 9.9 %collective-permute-start.1 = (f32[2,512]{1,0:T(2,128)S(1)}, f32[2,512]{1,0:T(2,128)S(1)}, u32[]{:S(2)}, u32[]{:S(2)}) collective-permute-start(f32[2,512]{1,0:T(2,128)S(1)} %slice.58), channel_id=1, source_target_pairs={{0,8},{8,16},{16,24},{1,9},{9,17},{17,25},{2,10},{10,18},{18,26},{... | collective-permute-start | bytes 12296 | tf_op jit(solution)/shard_map/ppermute | solution.py:21
Sparse Core Ops, SparseCore 0:
  12.3 134.1 all-gather.6
  148.0 11.8 all-gather.4
  162.7 97.2 all-gather.8
  262.6 90.7 all-gather.10
  361.7 10.2 reduce-scatter.1

commit v3 on v2

--- a/solution.py
+++ b/solution.py
@@ -19,6 +19,27 @@
     devices = range(lax.axis_size(axis))
     route = [(i - distance, i) for i in devices if i - distance in devices]
     return lax.ppermute(block, axis, route)
+
+
+def rotated(block, axis, distance):
+    count = lax.axis_size(axis)
+    return lax.ppermute(block, axis, [(i, (i + distance) % count) for i in range(count)])
+
+
+def permuted_columns(block, outer, inner):
+    outer_count, inner_count = lax.axis_size(outer), lax.axis_size(inner)
+    width = block.shape[1]
+    column = [block] + [rotated(block, outer, d) for d in range(1, outer_count)]
+    stack = jnp.stack(column)
+    stacks = [stack] + [rotated(stack, inner, d) for d in range(1, inner_count)]
+    whole = jnp.zeros((block.shape[0], outer_count * inner_count * width), block.dtype)
+    for e in range(inner_count):
+        inner_at = (lax.axis_index(inner) - e + inner_count) % inner_count
+        for d in range(outer_count):
+            outer_at = (lax.axis_index(outer) - d + outer_count) % outer_count
+            start = (outer_at * inner_count + inner_at) * width
+            whole = lax.dynamic_update_slice(whole, stacks[e][d], (0, start))
+    return whole
 
 
 def rms_rows(activations, gain_vector):
@@ -347,7 +368,7 @@
         * head_norm_gain.reshape(present_heads, HEAD_WIDTH)
     )
     state_mixed = state_mixed.reshape(sequence_rows, channels).astype(jnp.bfloat16)
-    out_whole = lax.all_gather(outgoing, ("sp", "fs"), axis=1, tiled=True)
+    out_whole = permuted_columns(outgoing, "sp", "fs")
     mixed = lax.psum_scatter(
         (
             jnp.dot(

time: 379 us -> 375 us (0.989)
  waiting for transfers between devices: 239 us -> 203 us
  local copies, waits for them, and re-layouts: 21.9 us -> 40.4 us
  starting transfers between devices: 26 us -> 36.3 us
    all_gather x1 -> x0, waiting for transfers between devices: 70.3 us -> none  [on_device(): out_whole = lax.all_gather(outgoing, ('sp', 'fs'), axis=1, tiled=True)]
    reduce_scatter x1, waiting for transfers between devices: 10.4 us -> 32.3 us  [on_device(): lax.psum_scatter(jnp.dot(jnp.concatenate([conv_mixed, state_mixed], axis=...]
    dynamic_update_slice x0 -> x16, local copies, waits for them, and re-layouts: none -> 15.8 us  [permuted_columns(): whole = lax.dynamic_update_slice(whole, stacks[e][d], (0, start))]
    ppermute x0 -> x6, waiting for transfers between devices: none -> 14.7 us  [rotated(): lax.ppermute(block, axis, [(i, (i + distance) % count) for i in range(cou...]
    ppermute x0 -> x6, starting transfers between devices: none -> 9.15 us  [rotated(): lax.ppermute(block, axis, [(i, (i + distance) % count) for i in range(cou...]
    all_gather x1, waiting for transfers between devices: 12.8 us -> 8.65 us  [on_device(): piece = lax.all_gather(normed, 'tp', axis=0, tiled=True)]
  transfers between devices with their start and end apart: 9 -> 14, of which waited for: 8 -> 9; matrix products, arithmetic and copies ran while one was open for 14% -> 17% of each run, Pallas kernels for 8% -> 8%
where the time goes in v3:
time: 375 us
  waiting for transfers between devices  203 us (54%)
  local copies, waits for them, and re-layouts  40.4 us (11%)
  matrix products  38.5 us (10%)
  starting transfers between devices  36.3 us (10%)
  Pallas kernels  31.7 us (8%)
  between operations  13.7 us (4%)
  other arithmetic  10.9 us (3%)
    all_gather x1, waiting for transfers between devices, on_device(): lax.all_gather(state_weights, ('sp', 'fs'), axis=0, tiled=True)  128 us
    reduce_scatter x1, waiting for transfers between devices, on_device(): lax.psum_scatter(jnp.dot(jnp.concatenate([conv_mixed, state_mixed], axis=...  32.3 us
    pallas_call x1, Pallas kernels, delta_mix(): pl.pallas_call(delta_kernel, grid=(rows // turn,), in_specs=[pl.BlockSpec...  31.7 us
    ppermute x4, starting transfers between devices, passed_along(): return lax.ppermute(block, axis, route)  27.1 us
    dot_general x2, matrix products, project(): jnp.dot(activations, weight, preferred_element_type=jnp.float32)  26.7 us
    ppermute x4, waiting for transfers between devices, passed_along(): return lax.ppermute(block, axis, route)  18.7 us
    dynamic_update_slice x16, local copies, waits for them, and re-layouts, permuted_columns(): whole = lax.dynamic_update_slice(whole, stacks[e][d], (0, start))  15.8 us
    ppermute x6, waiting for transfers between devices, rotated(): lax.ppermute(block, axis, [(i, (i + distance) % count) for i in range(cou...  14.7 us
  transfers between devices with their start and end apart: 14, of which 9 were waited for; matrix products, arithmetic and copies ran while one was open for 17% of the time, Pallas kernels for 8%

profile of v3, /device:TPU:0, one launch (start us, length us, event | category | flops | bytes accessed | tf_op | source)
XLA Modules:
  0.0 374.6 jit_solution(5396601788798408544)
XLA Ops:
  6.5 1.1 constant_dynamic-update-slice_fusion.4
  7.6 0.9 constant_dynamic-update-slice_fusion.3
  8.5 0.9 constant_dynamic-update-slice_fusion.2
  9.4 0.9 constant_dynamic-update-slice_fusion.1
  10.4 0.9 constant_dynamic-update-slice_fusion
  11.3 0.8 copy-done.4
  12.3 2.2 fusion.5
  14.5 2.6 fusion.7
  17.2 0.8 pad_maximum_fusion.2
  18.0 128.5 %all-gather.6.cloned.1.call-done = bf16[2048,2560]{1,0:T(8,128)(2,1)} async-done(((bf16[128,2560]{1,0:T(8,128)(2,1)}), bf16[2048,2560]{1,0:T(8,128)(2,1)}) %all-gather.6.cloned.1.call-update) | async-done | bytes 10485776 | tf_op jit(solution)/shard_map/all_gather | solution.py:328
  146.9 1.9 collective-permute-start.3
  148.8 2.4 collective-permute-start.4
  151.3 8.6 %all-gather.4.cloned.1.call-done = bf16[1024,2048]{1,0:T(8,128)(2,1)} async-done(((bf16[512,2048]{1,0:T(8,128)(2,1)}), bf16[1024,2048]{1,0:T(8,128)(2,1)}) %all-gather.4.cloned.1.call-update) | async-done | bytes 4194320 | tf_op jit(solution)/shard_map/all_gather | solution.py:327
  159.9 16.7 %convolution_convert_fusion.proj_ref = bf16[1024,2560]{1,0:T(8,128)(2,1)} fusion(bf16[1024,2048]{1,0:T(8,128)(2,1)} %all-gather.4.cloned.1.call-done, bf16[2048,2560]{1,0:T(8,128)(2,1)} %all-gather.6.cloned.1.call-done), kind=kOutput, calls=%fused_computation.7 | convolution fusion | flops 10740039680 | bytes 19922944 | tf_op jit(solution)/shard_map/dot_general | solution.py:52
  176.6 31.7 %shard_map.172 = (f32[1024,512]{1,0:T(8,128)}, bf16[1024,512]{1,0:T(8,128)(2,1)}, f32[4,256,128]{2,1,0:T(8,128)}) custom-call(bf16[1024,2560]{1,0:T(8,128)(2,1)} %convolution_convert_fusion.proj_ref, f32[1024,512]{1,0:T(8,128)} %bitcast.128, f32[1,512]{1,0:T(1,128)} %bitcast.129, f32[1,512]{1,0:T(1,128)} %bitcast.130), custom_call_target="tpu_custom_call" | custom-call | flops 2684354560 | bytes 10485760 | tf_op jit(solution)/shard_map/pallas_call | solution.py:255
  208.3 1.1 fusion.46
  210.6 2.9 copy.38
  213.5 36.4 %while.11 = (s32[]{:T(128)}, f32[8,64,64]{2,1,0:T(8,128)S(1)}, pred[]{:T(512)}, f32[8,64,64]{2,1,0:T(8,128)S(1)}, f32[8,64,64]{2,1,0:T(8,128)S(1)}, /*index=5*/f32[8,64,64]{2,1,0:T(8,128)S(1)}, s32[]{:T(128)}, s32[]{:T(128)}) while((s32[]{:T(128)}, f32[8,64,64]{2,1,0:T(8,128)S(1)}, pred[]{:T(512)}, f32[8,64,64]{2,1,0:T(8,128)S(1)}, ...), condition=%wide.region_2.3_spmd.clone, body=%wide.region_1.2_spmd.clone.sunk | while | flops 25329668 | bytes 1048712 | solution.py:353
  213.5 0.4 fusion.59
  213.9 3.7 collective-permute-start
  217.6 6.3 %collective-permute-done = bf16[8,64,64]{2,1,0:T(8,128)(2,1)S(1)} collective-permute-done((bf16[8,64,64]{2,1,0:T(8,128)(2,1)S(1)}, bf16[8,64,64]{2,1,0:T(8,128)(2,1)S(1)}, u32[]{:S(2)}, u32[]{:S(2)}) %collective-permute-start) | collective-permute-done | bytes 65568 | tf_op jit(solution)/shard_map/while/body/eval_jaxpr/ppermute | solution.py:21
  223.9 0.4 fusion.59
  224.3 5.8 %collective-permute-start = (bf16[8,64,64]{2,1,0:T(8,128)(2,1)S(1)}, bf16[8,64,64]{2,1,0:T(8,128)(2,1)S(1)}, u32[]{:S(2)}, u32[]{:S(2)}) collective-permute-start(bf16[8,64,64]{2,1,0:T(8,128)(2,1)S(1)} %fusion.59), channel_id=1, source_target_pairs={{0,8},{8,16},{16,24},{1,9},{9,17},{17,25},{2,10},{10,18},{18,26},{... | collective-permute-start | bytes 196616 | tf_op jit(solution)/shard_map/while/body/eval_jaxpr/ppermute | solution.py:21
  230.2 6.4 %collective-permute-done = bf16[8,64,64]{2,1,0:T(8,128)(2,1)S(1)} collective-permute-done((bf16[8,64,64]{2,1,0:T(8,128)(2,1)S(1)}, bf16[8,64,64]{2,1,0:T(8,128)(2,1)S(1)}, u32[]{:S(2)}, u32[]{:S(2)}) %collective-permute-start) | collective-permute-done | bytes 65568 | tf_op jit(solution)/shard_map/while/body/eval_jaxpr/ppermute | solution.py:21
  236.6 0.4 fusion.59
  237.0 7.3 %collective-permute-start = (bf16[8,64,64]{2,1,0:T(8,128)(2,1)S(1)}, bf16[8,64,64]{2,1,0:T(8,128)(2,1)S(1)}, u32[]{:S(2)}, u32[]{:S(2)}) collective-permute-start(bf16[8,64,64]{2,1,0:T(8,128)(2,1)S(1)} %fusion.59), channel_id=1, source_target_pairs={{0,8},{8,16},{16,24},{1,9},{9,17},{17,25},{2,10},{10,18},{18,26},{... | collective-permute-start | bytes 196616 | tf_op jit(solution)/shard_map/while/body/eval_jaxpr/ppermute | solution.py:21
  244.3 5.6 %collective-permute-done = bf16[8,64,64]{2,1,0:T(8,128)(2,1)S(1)} collective-permute-done((bf16[8,64,64]{2,1,0:T(8,128)(2,1)S(1)}, bf16[8,64,64]{2,1,0:T(8,128)(2,1)S(1)}, u32[]{:S(2)}, u32[]{:S(2)}) %collective-permute-start) | collective-permute-done | bytes 65568 | tf_op jit(solution)/shard_map/while/body/eval_jaxpr/ppermute | solution.py:21
  250.0 2.4 bitcast_add_fusion
  253.0 1.1 pad_maximum_fusion.1
  254.2 1.6 collective-permute-start.5
  255.8 1.6 mul.167
  257.3 2.9 copy.37
  260.2 1.6 sub.9
  261.8 2.9 copy.36
  264.7 1.8 copy.39
  266.5 2.7 broadcast_in_dim.7
  269.1 0.8 constant_dynamic-update-slice_fusion.8
  269.9 0.4 copy-done.3
  270.3 2.4 multiply_convert_fusion
  272.7 1.6 collective-permute-start.6
  274.3 1.5 collective-permute-start.7
  275.8 0.8 constant_dynamic-update-slice_fusion.7
  276.5 0.7 constant_dynamic-update-slice_fusion.6
  277.3 0.7 constant_dynamic-update-slice_fusion.5
  278.0 3.1 collective-permute-done.5
  281.1 1.7 fusion.31
  282.8 1.7 fusion.30
  284.5 1.7 fusion.29
  286.2 1.7 fusion.28
  287.9 11.6 %collective-permute-done.6 = bf16[4,1024,128]{2,1,0:T(8,128)(2,1)S(1)} collective-permute-done((bf16[4,1024,128]{2,1,0:T(8,128)(2,1)}, bf16[4,1024,128]{2,1,0:T(8,128)(2,1)S(1)}, u32[]{:S(2)}, u32[]{:S(2)}) %collective-permute-start.6) | collective-permute-done | bytes 1048608 | tf_op jit(solution)/shard_map/ppermute | solution.py:26
  299.5 0.8 fusion.27
  300.3 0.7 fusion.26
  301.0 0.7 fusion.25
  301.8 0.8 fusion.24
  302.5 0.8 fusion.23
  303.3 0.8 fusion.22
  304.1 0.7 fusion.21
  304.8 10.0 %convolution_convert_fusion.1 = bf16[1024,1536]{1,0:T(8,128)(2,1)S(1)} fusion(bf16[1024,2048]{1,0:T(8,128)(2,1)} %all-gather.4.cloned.1.call-done, bf16[2048,1536]{1,0:T(8,128)(2,1)} %all-gather.8.cloned.1.call-done), kind=kOutput, calls=%fused_computation.13 | convolution fusion | flops 6444023808 | bytes 13631488 | tf_op jit(solution)/shard_map/dot_general | solution.py:52
  315.1 10.3 %collective-permute-start.1 = (f32[2,512]{1,0:T(2,128)S(1)}, f32[2,512]{1,0:T(2,128)S(1)}, u32[]{:S(2)}, u32[]{:S(2)}) collective-permute-start(f32[2,512]{1,0:T(2,128)S(1)} %slice.106), channel_id=1, source_target_pairs={{0,8},{8,16},{16,24},{1,9},{9,17},{17,25},{2,10},{10,18},{18,26},{... | collective-permute-start | bytes 12296 | tf_op jit(solution)/shard_map/ppermute | solution.py:21
  325.4 0.8 fusion.20
  326.2 0.5 collective-permute-done.1
  326.7 0.8 fusion.13
  327.5 8.2 %convolution_convert_fusion.2 = bf16[1024,2048]{1,0:T(8,128)(2,1)} fusion(bf16[1024,2048]{1,0:T(8,128)(2,1)} %fusion.20, bf16[1024,512]{1,0:T(8,128)(2,1)S(1)} %multiply_convert_fusion, bf16[1024,512]{1,0:T(8,128)(2,1)S(1)} %fusion.13), kind=kOutput, calls=%fused_computation.14 | convolution fusion | flops 4301258752 | bytes 10485760 | tf_op jit(solution)/shard_map/dot_general | solution.py:374
  335.7 32.3 %reduce-scatter.2.cloned.1.call-done = bf16[512,2048]{1,0:T(8,128)(2,1)} async-done(((bf16[1024,2048]{1,0:T(8,128)(2,1)}), bf16[512,2048]{1,0:T(8,128)(2,1)}) %reduce-scatter.2.cloned.1.call-update) | async-done | bytes 2097168 | tf_op jit(solution)/shard_map/reduce_scatter | solution.py:372
  (59 shorter events, 2.6 us)
Async XLA Ops:
  6.5 8.0 %copy-start.1 = (bf16[1,512,2048]{2,1,0:T(8,128)(2,1)S(1)}, bf16[1,512,2048]{2,1,0:T(8,128)(2,1)}, u32[]{:S(2)}) copy-start(bf16[1,512,2048]{2,1,0:T(8,128)(2,1)} %param.20) | copy-start | bytes 6291460
  6.5 140.0 %all-gather.6.cloned.1.call-start = ((), (), s32[]{:S(2)}) async-start(), calls=%async_computation.2 | async-start | bytes 11141120 | tf_op jit(solution)/shard_map/all_gather | solution.py:328
  11.3 0.8 copy-start.4
  12.1 5.0 %copy-start.5 = (bf16[512,128]{1,0:T(8,128)(2,1)S(1)}, bf16[512,128]{1,0:T(8,128)(2,1)}, u32[]{:S(2)}) copy-start(bf16[512,128]{1,0:T(8,128)(2,1)} %param.37) | copy-start | bytes 393220
  12.2 5.0 %copy-start.6 = (bf16[512,128]{1,0:T(8,128)(2,1)S(1)}, bf16[512,128]{1,0:T(8,128)(2,1)}, u32[]{:S(2)}) copy-start(bf16[512,128]{1,0:T(8,128)(2,1)} %param.36) | copy-start | bytes 393220
  12.2 5.0 %copy-start.7 = (bf16[128,512]{1,0:T(8,128)(2,1)S(1)}, bf16[128,512]{1,0:T(8,128)(2,1)}, u32[]{:S(2)}) copy-start(bf16[128,512]{1,0:T(8,128)(2,1)} %param.24) | copy-start | bytes 393220
  12.2 5.0 %copy-start.8 = (bf16[128,512]{1,0:T(8,128)(2,1)S(1)}, bf16[128,512]{1,0:T(8,128)(2,1)}, u32[]{:S(2)}) copy-start(bf16[128,512]{1,0:T(8,128)(2,1)} %param.23) | copy-start | bytes 393220
  12.2 5.0 %copy-start.9 = (bf16[128,512]{1,0:T(8,128)(2,1)S(1)}, bf16[128,512]{1,0:T(8,128)(2,1)}, u32[]{:S(2)}) copy-start(bf16[128,512]{1,0:T(8,128)(2,1)} %param.22) | copy-start | bytes 393220
  12.2 147.7 %all-gather.4.cloned.1.call-start = ((), (), s32[]{:S(2)}) async-start(), calls=%async_computation.1 | async-start | bytes 6291456 | tf_op jit(solution)/shard_map/all_gather | solution.py:327
  14.5 132.3 %copy-start.10 = (f32[3,512]{1,0:T(4,128)S(1)}, f32[3,512]{1,0:T(4,128)}, u32[]{:S(2)}) copy-start(f32[3,512]{1,0:T(4,128)} %param.25) | copy-start | bytes 18436
  17.1 287.7 %all-gather.8.cloned.1.call-start = ((), (), s32[]{:S(2)}) async-start(), calls=%async_computation.3 | async-start | bytes 6684672 | tf_op jit(solution)/shard_map/all_gather | solution.py:338
  146.5 221.5 %reduce-scatter.2.cloned.1.call-start = ((), (), s32[]{:S(2)}) async-start(), calls=%async_computation.4 | async-start | bytes 6291456 | tf_op jit(solution)/shard_map/reduce_scatter | solution.py:372
  146.8 106.2 %collective-permute-start.2 = (bf16[1024,128]{1,0:T(8,128)(2,1)S(1)}, bf16[1024,128]{1,0:T(8,128)(2,1)S(1)}, u32[]{:S(2)}, u32[]{:S(2)}) collective-permute-start(bf16[1024,128]{1,0:T(8,128)(2,1)S(1)} %pad_maximum_fusion.3), channel_id=1, source_target_pairs={{0,8},{8,16},{16,24},{24,0},{1,9},{9,17},{17,25},{25,1},{2,10},{10... | collective-permute-start | bytes 786440 | tf_op jit(solution)/shard_map/ppermute | solution.py:26
  146.9 106.1 %collective-permute-start.3 = (bf16[1024,128]{1,0:T(8,128)(2,1)S(1)}, bf16[1024,128]{1,0:T(8,128)(2,1)S(1)}, u32[]{:S(2)}, u32[]{:S(2)}) collective-permute-start(bf16[1024,128]{1,0:T(8,128)(2,1)S(1)} %pad_maximum_fusion.3), channel_id=1, source_target_pairs={{0,16},{8,24},{16,0},{24,8},{1,17},{9,25},{17,1},{25,9},{2,18},{10... | collective-permute-start | bytes 786440 | tf_op jit(solution)/shard_map/ppermute | solution.py:26
  148.8 104.2 %collective-permute-start.4 = (bf16[1024,128]{1,0:T(8,128)(2,1)S(1)}, bf16[1024,128]{1,0:T(8,128)(2,1)S(1)}, u32[]{:S(2)}, u32[]{:S(2)}) collective-permute-start(bf16[1024,128]{1,0:T(8,128)(2,1)S(1)} %pad_maximum_fusion.3), channel_id=1, source_target_pairs={{0,24},{8,0},{16,8},{24,16},{1,25},{9,1},{17,9},{25,17},{2,26},{10... | collective-permute-start | bytes 786440 | tf_op jit(solution)/shard_map/ppermute | solution.py:26
  209.7 3.8 %copy-start = (f32[1,8,64,64]{3,2,1,0:T(8,128)S(1)}, f32[1,8,64,64]{3,2,1,0:T(8,128)}, u32[]{:S(2)}) copy-start(f32[1,8,64,64]{3,2,1,0:T(8,128)} %param.34) | copy-start | bytes 393220
  213.9 10.0 %collective-permute-start = (bf16[8,64,64]{2,1,0:T(8,128)(2,1)S(1)}, bf16[8,64,64]{2,1,0:T(8,128)(2,1)S(1)}, u32[]{:S(2)}, u32[]{:S(2)}) collective-permute-start(bf16[8,64,64]{2,1,0:T(8,128)(2,1)S(1)} %fusion.59), channel_id=1, source_target_pairs={{0,8},{8,16},{16,24},{1,9},{9,17},{17,25},{2,10},{10,18},{18,26},{... | collective-permute-start | bytes 196616 | tf_op jit(solution)/shard_map/while/body/eval_jaxpr/ppermute | solution.py:21
  224.3 12.2 %collective-permute-start = (bf16[8,64,64]{2,1,0:T(8,128)(2,1)S(1)}, bf16[8,64,64]{2,1,0:T(8,128)(2,1)S(1)}, u32[]{:S(2)}, u32[]{:S(2)}) collective-permute-start(bf16[8,64,64]{2,1,0:T(8,128)(2,1)S(1)} %fusion.59), channel_id=1, source_target_pairs={{0,8},{8,16},{16,24},{1,9},{9,17},{17,25},{2,10},{10,18},{18,26},{... | collective-permute-start | bytes 196616 | tf_op jit(solution)/shard_map/while/body/eval_jaxpr/ppermute | solution.py:21
  237.0 12.9 %collective-permute-start = (bf16[8,64,64]{2,1,0:T(8,128)(2,1)S(1)}, bf16[8,64,64]{2,1,0:T(8,128)(2,1)S(1)}, u32[]{:S(2)}, u32[]{:S(2)}) collective-permute-start(bf16[8,64,64]{2,1,0:T(8,128)(2,1)S(1)} %fusion.59), channel_id=1, source_target_pairs={{0,8},{8,16},{16,24},{1,9},{9,17},{17,25},{2,10},{10,18},{18,26},{... | collective-permute-start | bytes 196616 | tf_op jit(solution)/shard_map/while/body/eval_jaxpr/ppermute | solution.py:21
  254.2 26.9 %collective-permute-start.5 = (bf16[4,1024,128]{2,1,0:T(8,128)(2,1)}, bf16[4,1024,128]{2,1,0:T(8,128)(2,1)}, u32[]{:S(2)}, u32[]{:S(2)}) collective-permute-start(bf16[4,1024,128]{2,1,0:T(8,128)(2,1)} %pad_maximum_fusion.1), channel_id=1, source_target_pairs={{0,2},{2,4},{4,6},{6,0},{1,3},{3,5},{5,7},{7,1},{8,10},{10,12},{12... | collective-permute-start | bytes 3145736 | tf_op jit(solution)/shard_map/ppermute | solution.py:26
  264.7 5.2 %copy-start.11 = (f32[512]{0:T(512)S(1)}, f32[512]{0:T(512)}, u32[]{:S(2)}) copy-start(f32[512]{0:T(512)} %param.35) | copy-start | bytes 6148
  266.5 3.4 copy-start.2
  266.5 3.8 %copy-start.3 = (f32[1024,512]{1,0:T(8,128)S(1)}, f32[1024,512]{1,0:T(8,128)}, u32[]{:S(2)}) copy-start(f32[1024,512]{1,0:T(8,128)} %copy.36) | copy-start | bytes 6291460
  272.7 26.8 %collective-permute-start.6 = (bf16[4,1024,128]{2,1,0:T(8,128)(2,1)}, bf16[4,1024,128]{2,1,0:T(8,128)(2,1)S(1)}, u32[]{:S(2)}, u32[]{:S(2)}) collective-permute-start(bf16[4,1024,128]{2,1,0:T(8,128)(2,1)} %pad_maximum_fusion.1), channel_id=1, source_target_pairs={{0,4},{2,6},{4,0},{6,2},{1,5},{3,7},{5,1},{7,3},{8,12},{10,14},{12... | collective-permute-start | bytes 3145736 | tf_op jit(solution)/shard_map/ppermute | solution.py:26
  274.3 28.3 %collective-permute-start.7 = (bf16[4,1024,128]{2,1,0:T(8,128)(2,1)}, bf16[4,1024,128]{2,1,0:T(8,128)(2,1)S(1)}, u32[]{:S(2)}, u32[]{:S(2)}) collective-permute-start(bf16[4,1024,128]{2,1,0:T(8,128)(2,1)} %pad_maximum_fusion.1), channel_id=1, source_target_pairs={{0,6},{2,0},{4,2},{6,4},{1,7},{3,1},{5,3},{7,5},{8,14},{10,8},{12,... | collective-permute-start | bytes 3145736 | tf_op jit(solution)/shard_map/ppermute | solution.py:26
  315.1 11.6 %collective-permute-start.1 = (f32[2,512]{1,0:T(2,128)S(1)}, f32[2,512]{1,0:T(2,128)S(1)}, u32[]{:S(2)}, u32[]{:S(2)}) collective-permute-start(f32[2,512]{1,0:T(2,128)S(1)} %slice.106), channel_id=1, source_target_pairs={{0,8},{8,16},{16,24},{1,9},{9,17},{17,25},{2,10},{10,18},{18,26},{... | collective-permute-start | bytes 12296 | tf_op jit(solution)/shard_map/ppermute | solution.py:21
Sparse Core Ops, SparseCore 0:
  12.3 134.1 all-gather.5
  148.0 11.8 all-gather.3
  162.7 97.6 all-gather.7
  335.8 32.1 reduce-scatter.1
